TPU v7x, 32 devices: a whole 2x2x4 slice. The times are simulated.
32 devices in a mesh: sp: 8 (over z, core), tp: 4 (over y, x).
Axes of the slice: x: 2, y: 2, z: 4, core: 2. Of those that a mesh axis runs over, the one named last changes fastest.
Arguments:
- layer_input: bfloat16 [8192, 4096], P('sp', 'tp'), may hold values from -6 to 6
- key_weight: bfloat16 [4096, 4096], P(None, 'tp'), may hold values from -0.09375 to 0.09375
- value_weight: bfloat16 [4096, 4096], P(None, 'tp'), may hold values from -0.09375 to 0.09375
- decay_exponent: float32 [32], P('tp'), may hold values from -0.077 to -0.00016845703, as said below
- query_new: bfloat16 [2, 4096], P(None, 'tp'), may hold values from -6 to 6
- key_new: bfloat16 [2, 4096], P(None, 'tp'), may hold values from -6 to 6
- value_new: bfloat16 [2, 4096], P(None, 'tp'), may hold values from -6 to 6
- norm_gain: float32 [4096], P('tp'), may hold values from 0.1 to 1.9
Outputs:
- state_cache: bfloat16 [2, 32, 128, 128], P(None, 'tp', 'sp')
- first_read: bfloat16 [2, 4096], P(None, 'tp')
Inputs may be any that keep to these rules, and one draw needn't show every extreme that they name: decay_exponent is negative.
All inputs are finite; a program needn't handle non-finite values.
Results may differ from a plain program's by a relative error of at most 0.011.
Values may be sent and summed in bfloat16 or wider, within the bound.
A program may use at most 64 MiB of HBM per device.

v0:
```python
import functools
import math

import jax
import jax.numpy as jnp
import numpy as np
from jax import lax
from jax.experimental import pallas as pl
from jax.experimental.pallas import tpu as pltpu
from jax.sharding import PartitionSpec as P

SEQS = 2
CHUNKS = 8
MESH = pl.DeviceIdType.MESH
F32 = jnp.float32
BF16 = jnp.bfloat16


def gather_kernel(
    side, seq_span, chunks,
    decay_hbm, inv_hbm, query_hbm, key_hbm, value_hbm, gain_hbm, x_ref, wk_ref, wv_ref,
    cache_ref, first_ref,
    decay_ref, inv_ref, query_ref, key_ref, value_ref, gain_ref,
    gx, wk, wv, cosine, sine, acc_k, acc_v,
    state_ref, query_wide, own_term, factor, staged, landed, read, reads,
    send_sem, recv_sem, local_sem, state_send, state_recv, read_send, read_recv,
):
    tokens, feats = x_ref.shape
    rows = tokens // chunks
    half = rows // 2
    heads, width, vwidth = state_ref.shape
    pair = next(p for p in (4, 2, 1) if heads % p == 0)
    me = lax.axis_index("tp")
    my_y, my_x = me // side, lax.rem(me, side)
    sp_place = lax.axis_index("sp")
    sp_size = landed.shape[0]
    kept = landed.shape[2]
    groups = heads // pair
    sp_peers = [lax.rem(sp_place + d, sp_size) for d in range(1, sp_size)]

    def x_peer(d):
        return my_y * side + lax.rem(my_x + d, side)

    def y_peer(d):
        return lax.rem(my_y + d, side) * side + my_x

    x_peers = [x_peer(d) for d in range(1, side)]
    y_peers = [y_peer(d) for d in range(1, side)]

    barrier = pltpu.get_barrier_semaphore()
    for peer in x_peers + y_peers:
        pl.semaphore_signal(barrier, inc=1, device_id={"tp": peer}, device_id_type=MESH)
    for peer in sp_peers:
        pl.semaphore_signal(barrier, inc=1, device_id={"sp": peer}, device_id_type=MESH)
    pl.semaphore_wait(barrier, 2 * (side - 1) + sp_size - 1)

    def span(c, part):
        return pl.ds(pl.multiple_of(c * rows + part * half, half), half)

    def remote(c, slot, block, part, target, from_input):
        where = span(c, part)
        return pltpu.make_async_remote_copy(
            src_ref=x_ref.at[where] if from_input else gx.at[block, where],
            dst_ref=gx.at[block, where],
            send_sem=send_sem.at[c, slot],
            recv_sem=recv_sem.at[c, block, part],
            device_id={"tp": target},
            device_id_type=MESH,
        )

    def own_copies(c):
        out, slot = [], 0
        for first in (True, False):
            for part, peers in ((0, x_peers), (1, y_peers)):
                for peer in peers:
                    out.append(remote(c, slot, me, part if first else 1 - part, peer, True))
                    slot += 1
        return out

    def relay_copies(c):
        out, slot = [], 4 * (side - 1)
        for part, sources, peers in ((0, x_peers, y_peers), (1, y_peers, x_peers)):
            for source in sources:
                for peer in peers:
                    out.append(remote(c, slot, source, part, peer, False))
                    slot += 1
        return out

    def arrived(c, block, part):
        remote(c, 0, block, part, x_peers[0], False).wait_recv()

    late_blocks = [
        lax.rem(my_y + dy, side) * side + lax.rem(my_x + dx, side)
        for dy in range(1, side)
        for dx in range(1, side)
    ]

    def wait_early(c):
        for block in x_peers + y_peers:
            for part in range(2):
                arrived(c, block, part)

    def wait_late(c):
        for block in late_blocks:
            for part in range(2):
                arrived(c, block, part)

    def start_all(copies):
        for copy in copies:
            copy.start()

    start_all(own_copies(0))
    if chunks > 1:
        start_all(own_copies(1))

    small = [
        pltpu.make_async_copy(source, target, local_sem.at[3 + i])
        for i, (source, target) in enumerate((
            (decay_hbm, decay_ref), (inv_hbm, inv_ref), (query_hbm, query_ref),
            (key_hbm, key_ref), (value_hbm, value_ref), (gain_hbm, gain_ref),
        ))
    ]
    for copy in small:
        copy.start()
    local = [
        pltpu.make_async_copy(x_ref, gx.at[me], local_sem.at[0]),
        pltpu.make_async_copy(wk_ref, wk, local_sem.at[1]),
        pltpu.make_async_copy(wv_ref, wv, local_sem.at[2]),
    ]
    for copy in local:
        copy.start()
    state_ref[...] = jnp.zeros_like(state_ref)
    for copy in small:
        copy.wait()
    base = lax.rem(sp_place, seq_span) * tokens

    def table(c, _):
        at = pl.ds(pl.multiple_of(c * half, half), half)
        place = (base + c * half + lax.broadcasted_iota(jnp.int32, (half, width), 0)).astype(F32)
        angle = place * inv_ref[...]
        low = lax.broadcasted_iota(jnp.int32, (half, width), 1) < width // 2
        sin = jnp.sin(angle)
        cosine[at, :] = jnp.cos(angle)
        sine[at, :] = jnp.where(low, -sin, sin)
        return 0

    lax.fori_loop(0, 2 * chunks, table, 0)

    prompt = sp_place // seq_span
    diagonal = lax.broadcasted_iota(jnp.int32, (width, width), 0) == lax.broadcasted_iota(
        jnp.int32, (width, width), 1
    )
    ones = jnp.ones((width, vwidth), BF16)
    queries = query_ref[...].astype(F32)
    next_keys = key_ref[...].astype(F32)
    next_values = value_ref[...].astype(F32)
    for h in range(heads):
        cols = slice(h * width, (h + 1) * width)
        vcols = slice(h * vwidth, (h + 1) * vwidth)
        mine = jnp.zeros((1, width), F32)
        for s in range(SEQS):
            mine = jnp.where(prompt == s, queries[s:s + 1, cols], mine)
            score = jnp.sum(
                queries[s:s + 1, cols] * next_keys[s:s + 1, cols], axis=1, keepdims=True
            )
            own_term[s, h] = score * next_values[s:s + 1, vcols]
        spread = jnp.where(diagonal, jnp.broadcast_to(mine, (width, width)), 0.0).astype(BF16)
        query_wide[h] = jnp.dot(spread, ones, preferred_element_type=F32)
        factor[h] = jnp.exp(jnp.full((1, vwidth), decay_ref[h], F32))

    def state_copies(g):
        piece = pl.ds(g * pair, pair)
        return [
            pltpu.make_async_remote_copy(
                src_ref=staged.at[peer, piece],
                dst_ref=landed.at[sp_place, piece],
                send_sem=state_send.at[g, d],
                recv_sem=state_recv.at[g, sp_place],
                device_id={"sp": peer},
                device_id_type=MESH,
            )
            for d, peer in enumerate(sp_peers)
        ]

    def read_copies():
        return [
            pltpu.make_async_remote_copy(
                src_ref=read,
                dst_ref=reads.at[sp_place],
                send_sem=read_send.at[d],
                recv_sem=read_recv.at[sp_place],
                device_id={"sp": peer},
                device_id_type=MESH,
            )
            for d, peer in enumerate(sp_peers)
        ]

    for copy in local:
        copy.wait()

    def partial(c, blocks, w, cols):
        at = pl.ds(pl.multiple_of(c * rows, rows), rows)
        total = None
        for block in blocks:
            depth = pl.ds(pl.multiple_of(block * feats, feats), feats)
            term = jnp.dot(gx[block, at, :], w[depth, cols], preferred_element_type=F32)
            total = term if total is None else total + term
        return total

    early_blocks = [me] + x_peers + y_peers

    def finish(c, blocks, carry):
        at = pl.ds(pl.multiple_of(c * rows, rows), rows)
        distance = (seq_span * tokens - 1 - base - c * rows) - lax.broadcasted_iota(
            jnp.int32, (rows, width), 0
        )
        distance = distance.astype(F32)

        def step(g, _):
            kcols = pl.ds(pl.multiple_of(g * pair * width, pair * width), pair * width)
            vcols = pl.ds(pl.multiple_of(g * pair * vwidth, pair * vwidth), pair * vwidth)
            k = partial(c, blocks, wk, kcols)
            v = partial(c, blocks, wv, vcols)
            if carry:
                k = k + acc_k[:, kcols]
                v = v + acc_v[:, vcols]
            v = v.astype(BF16)
            for j in range(pair):
                kh = k[:, j * width:(j + 1) * width]
                turned = kh * cosine[at, :] + pltpu.roll(kh, width // 2, 1) * sine[at, :]
                keys = (turned * width ** (-0.5)).astype(BF16).astype(F32)
                weighted = (keys * jnp.exp(decay_ref[g * pair + j] * distance)).astype(BF16)
                state_ref[g * pair + j] += lax.dot_general(
                    weighted, v[:, j * vwidth:(j + 1) * vwidth],
                    (((0,), (0,)), ((), ())), preferred_element_type=F32,
                )
            if carry:
                for j in range(pair):
                    h = g * pair + j
                    held = state_ref[h]
                    for d in range(sp_size):
                        staged[d, h] = held[d * kept:(d + 1) * kept, :].astype(BF16)
                    read[h] = jnp.sum(query_wide[h] * held, axis=0, keepdims=True)
                start_all(state_copies(g))
            return 0

        lax.fori_loop(0, groups, step, 0)

    def round_trip(c, _):
        wait_early(c)
        start_all(relay_copies(c))

        @pl.when(c + 2 < chunks)
        def _():
            start_all(own_copies(c + 2))

        @pl.when(c > 0)
        def _():
            wait_late(c - 1)
            finish(c - 1, early_blocks + late_blocks, False)

        return 0

    lax.fori_loop(0, chunks, round_trip, 0)
    last = chunks - 1

    def early(g, _):
        kcols = pl.ds(pl.multiple_of(g * pair * width, pair * width), pair * width)
        vcols = pl.ds(pl.multiple_of(g * pair * vwidth, pair * vwidth), pair * vwidth)
        acc_k[:, kcols] = partial(last, early_blocks, wk, kcols)
        acc_v[:, vcols] = partial(last, early_blocks, wv, vcols)
        return 0

    lax.fori_loop(0, heads // pair, early, 0)
    wait_late(last)
    finish(last, late_blocks, True)

    start_all(read_copies())
    landed[sp_place] = staged[sp_place]
    reads[sp_place] = read[...]

    for d, peer in enumerate(sp_peers):
        pltpu.make_async_remote_copy(
            src_ref=read, dst_ref=reads.at[peer], send_sem=read_send.at[d],
            recv_sem=read_recv.at[peer], device_id={"sp": peer}, device_id_type=MESH,
        ).wait_recv()
        for g in range(groups):
            piece = pl.ds(g * pair, pair)
            pltpu.make_async_remote_copy(
                src_ref=staged.at[peer, piece], dst_ref=landed.at[peer, piece],
                send_sem=state_send.at[g, d], recv_sem=state_recv.at[g, peer],
                device_id={"sp": peer}, device_id_type=MESH,
            ).wait_recv()

    row = lax.broadcasted_iota(jnp.int32, (SEQS, heads * vwidth), 0)
    out = jnp.zeros((SEQS, heads * vwidth), F32)
    for s in range(SEQS):
        members = range(s * seq_span, (s + 1) * seq_span)
        carried = functools.reduce(jnp.add, [reads[m] for m in members])
        mixed = factor[...] * carried + own_term[s]
        normed = mixed * lax.rsqrt(jnp.mean(mixed * mixed, axis=2, keepdims=True) + 1e-06)
        line = jnp.concatenate([normed[h] for h in range(heads)], axis=1) * gain_ref[...]
        out = jnp.where(row == s, jnp.broadcast_to(line, out.shape), out)
        for h in range(heads):
            cache_ref[s, h] = functools.reduce(
                jnp.add, [landed[m, h].astype(F32) for m in members]
            ).astype(BF16)
    first_ref[...] = out.astype(BF16)

    for copy in read_copies():
        copy.wait_send()
    for g in range(groups):
        for copy in state_copies(g):
            copy.wait_send()

    def drain(c, _):
        for copy in own_copies(c) + relay_copies(c):
            copy.wait_send()
        return 0

    lax.fori_loop(0, chunks, drain, 0)


def settle(cache_ref, first_ref, cache_out, first_out):
    cache_out[...] = cache_ref[...]
    first_out[...] = first_ref[...]


def on_device(
    layer_input, key_weight, value_weight, decay_exponent, query_new, key_new, value_new, norm_gain
):
    tokens, feats = layer_input.shape
    parts = lax.axis_size("tp")
    sp_size = lax.axis_size("sp")
    seq_span = sp_size // SEQS
    side = math.isqrt(parts)
    heads = decay_exponent.shape[0]
    width = key_weight.shape[1] // heads
    vwidth = value_weight.shape[1] // heads
    kept = width // sp_size
    groups = heads // next(p for p in (4, 2, 1) if heads % p == 0)
    steps = np.linspace(0.0, 1.0, width // 2, dtype=np.float32)
    inverse = (np.float32(1.0) / np.power(np.float32(10000.0), steps)).astype(np.float32)
    inverse = jnp.asarray(np.concatenate([inverse, inverse])[None, :])
    sends = 4 * (side - 1) + 2 * (side - 1) ** 2
    anywhere = pl.BlockSpec(memory_space=pl.ANY)
    vmem = pl.BlockSpec(memory_space=pltpu.VMEM)
    rows = tokens // CHUNKS
    state_cache, first_read = pl.pallas_call(
        functools.partial(gather_kernel, side, seq_span, CHUNKS),
        out_shape=(
            jax.ShapeDtypeStruct((SEQS, heads, kept, vwidth), BF16),
            jax.ShapeDtypeStruct((SEQS, heads * vwidth), BF16),
        ),
        in_specs=[anywhere] * 9,
        out_specs=(vmem, vmem),
        scratch_shapes=[
            pltpu.SMEM((heads,), F32),
            pltpu.VMEM(inverse.shape, F32),
            pltpu.VMEM(query_new.shape, BF16),
            pltpu.VMEM(key_new.shape, BF16),
            pltpu.VMEM(value_new.shape, BF16),
            pltpu.VMEM((1, heads * vwidth), F32),
            pltpu.VMEM((parts, tokens, feats), BF16),
            pltpu.VMEM(key_weight.shape, BF16),
            pltpu.VMEM(value_weight.shape, BF16),
            pltpu.VMEM((tokens, width), F32),
            pltpu.VMEM((tokens, width), F32),
            pltpu.VMEM((rows, heads * width), F32),
            pltpu.VMEM((rows, heads * vwidth), F32),
            pltpu.VMEM((heads, width, vwidth), F32),
            pltpu.VMEM((heads, width, vwidth), F32),
            pltpu.VMEM((SEQS, heads, 1, vwidth), F32),
            pltpu.VMEM((heads, 1, vwidth), F32),
            pltpu.VMEM((sp_size, heads, kept, vwidth), BF16),
            pltpu.VMEM((sp_size, heads, kept, vwidth), BF16),
            pltpu.VMEM((heads, 1, vwidth), F32),
            pltpu.VMEM((sp_size, heads, 1, vwidth), F32),
            pltpu.SemaphoreType.DMA((CHUNKS, sends)),
            pltpu.SemaphoreType.DMA((CHUNKS, parts, 2)),
            pltpu.SemaphoreType.DMA((9,)),
            pltpu.SemaphoreType.DMA((groups, sp_size - 1)),
            pltpu.SemaphoreType.DMA((groups, sp_size)),
            pltpu.SemaphoreType.DMA((sp_size - 1,)),
            pltpu.SemaphoreType.DMA((sp_size,)),
        ],
        compiler_params=pltpu.CompilerParams(
            collective_id=0, has_side_effects=True, vmem_limit_bytes=62 * 1024 * 1024
        ),
    )(
        decay_exponent, inverse, query_new, key_new, value_new, norm_gain.reshape(1, -1),
        layer_input, key_weight, value_weight,
    )
    return pl.pallas_call(
        settle,
        out_shape=(
            jax.ShapeDtypeStruct(state_cache.shape, BF16),
            jax.ShapeDtypeStruct(first_read.shape, BF16),
        ),
        in_specs=[vmem, vmem],
        out_specs=(vmem, vmem),
    )(state_cache, first_read)


def solution(mesh):
    in_specs = (
        P("sp", "tp"),
        P(None, "tp"),
        P(None, "tp"),
        P("tp"),
        P(None, "tp"),
        P(None, "tp"),
        P(None, "tp"),
        P("tp"),
    )
    out_specs = (P(None, "tp", "sp", None), P(None, "tp"))
    return jax.shard_map(
        on_device, mesh=mesh, in_specs=in_specs, out_specs=out_specs, check_vma=False
    )
```

profile of v0, /device:TPU:0, one launch (start us, length us, event | category | flops | bytes accessed | tf_op | source)
XLA Modules:
  0.0 89.5 jit_solution(5855808058012538349)
XLA Ops:
  0.6 87.4 %shard_map.104 = (bf16[2,8,16,128]{3,2,1,0:T(8,128)(2,1)}, bf16[2,1024]{1,0:T(2,128)(2,1)}) custom-call(f32[8]{0:T(128)} %decay_hbm.1, f32[1,128]{1,0:T(1,128)} %constant.2.clone.inv_hbm, bf16[2,1024]{1,0:T(2,128)(2,1)} %query_hbm.1, bf16[2,1024]{1,0:T(2,128)(2,1)} %key_hbm.1, bf16[2,1024]{1,0:T(2,128)(2,1)} %value_hbm.1, f32[1,1024]{1,0:T(1,128)} %bitcast.1, ...), custom_call_target="tpu_custom_call" | custom-call | tf_op jit(solution)/shard_map/pallas_call | solution.py:349
  88.0 1.5 %shard_map.105 = (bf16[2,8,16,128]{3,2,1,0:T(8,128)(2,1)}, bf16[2,1024]{1,0:T(2,128)(2,1)}) custom-call(bf16[2,8,16,128]{3,2,1,0:T(8,128)(2,1)} %get-tuple-element.4.cache_ref, bf16[2,1024]{1,0:T(2,128)(2,1)} %get-tuple-element.5.first_ref), custom_call_target="tpu_custom_call" | custom-call | tf_op jit(solution)/shard_map/pallas_call | solution.py:394
where the time goes:
time: 89.7 us; the launch traced here: 89.5 us
  Pallas kernels  88.9 us (99%)
    pallas_call x1, Pallas kernels, on_device(): pl.pallas_call(functools.partial(gather_kernel, side, seq_span, CHUNKS),...  87.4 us

commit v1 on v0

--- a/solution.py
+++ b/solution.py
@@ -11,6 +11,8 @@
 
 SEQS = 2
 CHUNKS = 8
+LEAD = 1
+VMEM_KIB = 48 * 1024
 MESH = pl.DeviceIdType.MESH
 F32 = jnp.float32
 BF16 = jnp.bfloat16
@@ -23,7 +25,7 @@
     decay_ref, inv_ref, query_ref, key_ref, value_ref, gain_ref,
     gx, wk, wv, cosine, sine, acc_k, acc_v,
     state_ref, query_wide, own_term, factor, staged, landed, read, reads,
-    send_sem, recv_sem, local_sem, state_send, state_recv, read_send, read_recv,
+    send_sem, recv_sem, local_sem, state_send, state_recv, read_send, read_recv, go_sem,
 ):
     tokens, feats = x_ref.shape
     rows = tokens // chunks
@@ -36,7 +38,16 @@
     sp_size = landed.shape[0]
     kept = landed.shape[2]
     groups = heads // pair
-    sp_peers = [lax.rem(sp_place + d, sp_size) for d in range(1, sp_size)]
+    core = lax.rem(sp_place, 2)
+
+    def mirror(m):
+        place, bit = 0, 1
+        while bit < sp_size:
+            flag = lax.rem(sp_place // bit + (m // bit) % 2, 2)
+            place, bit = place + flag * bit, bit * 2
+        return place
+
+    sp_peers = [mirror(m) for m in range(sp_size - 1, 0, -1)]
 
     def x_peer(d):
         return my_y * side + lax.rem(my_x + d, side)
@@ -47,6 +58,8 @@
     x_peers = [x_peer(d) for d in range(1, side)]
     y_peers = [y_peer(d) for d in range(1, side)]
 
+    fetch = pltpu.make_async_copy(x_ref, gx.at[me], local_sem.at[0])
+    fetch.start()
     barrier = pltpu.get_barrier_semaphore()
     for peer in x_peers + y_peers:
         pl.semaphore_signal(barrier, inc=1, device_id={"tp": peer}, device_id_type=MESH)
@@ -57,10 +70,10 @@
     def span(c, part):
         return pl.ds(pl.multiple_of(c * rows + part * half, half), half)
 
-    def remote(c, slot, block, part, target, from_input):
+    def remote(c, slot, block, part, target):
         where = span(c, part)
         return pltpu.make_async_remote_copy(
-            src_ref=x_ref.at[where] if from_input else gx.at[block, where],
+            src_ref=gx.at[block, where],
             dst_ref=gx.at[block, where],
             send_sem=send_sem.at[c, slot],
             recv_sem=recv_sem.at[c, block, part],
@@ -68,26 +81,27 @@
             device_id_type=MESH,
         )
 
-    def own_copies(c):
-        out, slot = [], 0
-        for first in (True, False):
-            for part, peers in ((0, x_peers), (1, y_peers)):
-                for peer in peers:
-                    out.append(remote(c, slot, me, part if first else 1 - part, peer, True))
-                    slot += 1
+    fan = 2 * (side - 1)
+
+    def own_copies(c, wave):
+        out, slot = [], wave * fan
+        for peers, part in ((x_peers, wave), (y_peers, 1 - wave)):
+            for peer in peers:
+                out.append(remote(c, slot, me, part, peer))
+                slot += 1
         return out
 
     def relay_copies(c):
-        out, slot = [], 4 * (side - 1)
+        out, slot = [], 2 * fan
         for part, sources, peers in ((0, x_peers, y_peers), (1, y_peers, x_peers)):
             for source in sources:
                 for peer in peers:
-                    out.append(remote(c, slot, source, part, peer, False))
+                    out.append(remote(c, slot, source, part, peer))
                     slot += 1
         return out
 
     def arrived(c, block, part):
-        remote(c, 0, block, part, x_peers[0], False).wait_recv()
+        remote(c, 0, block, part, x_peers[0]).wait_recv()
 
     late_blocks = [
         lax.rem(my_y + dy, side) * side + lax.rem(my_x + dx, side)
@@ -95,10 +109,11 @@
         for dx in range(1, side)
     ]
 
-    def wait_early(c):
-        for block in x_peers + y_peers:
-            for part in range(2):
-                arrived(c, block, part)
+    def wait_wave(c, wave):
+        for block in x_peers:
+            arrived(c, block, wave)
+        for block in y_peers:
+            arrived(c, block, 1 - wave)
 
     def wait_late(c):
         for block in late_blocks:
@@ -109,9 +124,25 @@
         for copy in copies:
             copy.start()
 
-    start_all(own_copies(0))
-    if chunks > 1:
-        start_all(own_copies(1))
+    def drain(copies):
+        for copy in copies:
+            copy.wait_send()
+
+    fetch.wait()
+
+    @pl.when(core == 1)
+    def _():
+        pl.semaphore_wait(go_sem, 1)
+
+    def send_wave(wave):
+        def body(c, _):
+            start_all(own_copies(c, wave))
+            return 0
+
+        lax.fori_loop(0, chunks, body, 0)
+
+    send_wave(0)
+    send_wave(1)
 
     small = [
         pltpu.make_async_copy(source, target, local_sem.at[3 + i])
@@ -123,13 +154,28 @@
     for copy in small:
         copy.start()
     local = [
-        pltpu.make_async_copy(x_ref, gx.at[me], local_sem.at[0]),
         pltpu.make_async_copy(wk_ref, wk, local_sem.at[1]),
         pltpu.make_async_copy(wv_ref, wv, local_sem.at[2]),
     ]
     for copy in local:
         copy.start()
     state_ref[...] = jnp.zeros_like(state_ref)
+
+    def pass_on(c):
+        wait_wave(c, 0)
+        start_all(relay_copies(c))
+
+    def pass_on_loop(c, _):
+        pass_on(c)
+        return 0
+
+    lead = min(LEAD, chunks)
+    lax.fori_loop(0, lead, pass_on_loop, 0)
+
+    @pl.when(core == 0)
+    def _():
+        pl.semaphore_signal(go_sem, inc=1, device_id={"sp": sp_place + 1}, device_id_type=MESH)
+
     for copy in small:
         copy.wait()
     base = lax.rem(sp_place, seq_span) * tokens
@@ -209,7 +255,22 @@
 
     early_blocks = [me] + x_peers + y_peers
 
-    def finish(c, blocks, carry):
+    def early(c, _):
+        wait_wave(c, 1)
+        at = pl.ds(pl.multiple_of(c * rows, rows), rows)
+
+        def step(g, _):
+            kcols = pl.ds(pl.multiple_of(g * pair * width, pair * width), pair * width)
+            vcols = pl.ds(pl.multiple_of(g * pair * vwidth, pair * vwidth), pair * vwidth)
+            acc_k[at, kcols] = partial(c, early_blocks, wk, kcols)
+            acc_v[at, vcols] = partial(c, early_blocks, wv, vcols)
+            return 0
+
+        lax.fori_loop(0, groups, step, 0)
+        return 0
+
+    def finish(c, last):
+        wait_late(c)
         at = pl.ds(pl.multiple_of(c * rows, rows), rows)
         distance = (seq_span * tokens - 1 - base - c * rows) - lax.broadcasted_iota(
             jnp.int32, (rows, width), 0
@@ -219,11 +280,8 @@
         def step(g, _):
             kcols = pl.ds(pl.multiple_of(g * pair * width, pair * width), pair * width)
             vcols = pl.ds(pl.multiple_of(g * pair * vwidth, pair * vwidth), pair * vwidth)
-            k = partial(c, blocks, wk, kcols)
-            v = partial(c, blocks, wv, vcols)
-            if carry:
-                k = k + acc_k[:, kcols]
-                v = v + acc_v[:, vcols]
+            k = partial(c, late_blocks, wk, kcols) + acc_k[at, kcols]
+            v = partial(c, late_blocks, wv, vcols) + acc_v[at, vcols]
             v = v.astype(BF16)
             for j in range(pair):
                 kh = k[:, j * width:(j + 1) * width]
@@ -234,7 +292,7 @@
                     weighted, v[:, j * vwidth:(j + 1) * vwidth],
                     (((0,), (0,)), ((), ())), preferred_element_type=F32,
                 )
-            if carry:
+            if last:
                 for j in range(pair):
                     h = g * pair + j
                     held = state_ref[h]
@@ -246,38 +304,32 @@
 
         lax.fori_loop(0, groups, step, 0)
 
-    def round_trip(c, _):
-        wait_early(c)
-        start_all(relay_copies(c))
-
-        @pl.when(c + 2 < chunks)
-        def _():
-            start_all(own_copies(c + 2))
-
-        @pl.when(c > 0)
-        def _():
-            wait_late(c - 1)
-            finish(c - 1, early_blocks + late_blocks, False)
-
+    def finish_loop(c, _):
+        finish(c, False)
         return 0
 
-    lax.fori_loop(0, chunks, round_trip, 0)
-    last = chunks - 1
-
-    def early(g, _):
-        kcols = pl.ds(pl.multiple_of(g * pair * width, pair * width), pair * width)
-        vcols = pl.ds(pl.multiple_of(g * pair * vwidth, pair * vwidth), pair * vwidth)
-        acc_k[:, kcols] = partial(last, early_blocks, wk, kcols)
-        acc_v[:, vcols] = partial(last, early_blocks, wv, vcols)
+    def drain_wave(wave):
+        def body(c, _):
+            drain(own_copies(c, wave))
+            return 0
+
+        lax.fori_loop(0, chunks, body, 0)
+
+    def drain_relay(c, _):
+        drain(relay_copies(c))
         return 0
 
-    lax.fori_loop(0, heads // pair, early, 0)
-    wait_late(last)
-    finish(last, late_blocks, True)
+    lax.fori_loop(lead, chunks, pass_on_loop, 0)
+    lax.fori_loop(0, chunks, early, 0)
+    lax.fori_loop(0, chunks - 1, finish_loop, 0)
+    drain_wave(0)
+    drain_wave(1)
+    finish(chunks - 1, True)
 
     start_all(read_copies())
     landed[sp_place] = staged[sp_place]
     reads[sp_place] = read[...]
+    lax.fori_loop(0, chunks, drain_relay, 0)
 
     for d, peer in enumerate(sp_peers):
         pltpu.make_async_remote_copy(
@@ -312,13 +364,6 @@
     for g in range(groups):
         for copy in state_copies(g):
             copy.wait_send()
-
-    def drain(c, _):
-        for copy in own_copies(c) + relay_copies(c):
-            copy.wait_send()
-        return 0
-
-    lax.fori_loop(0, chunks, drain, 0)
 
 
 def settle(cache_ref, first_ref, cache_out, first_out):
@@ -343,9 +388,15 @@
     inverse = (np.float32(1.0) / np.power(np.float32(10000.0), steps)).astype(np.float32)
     inverse = jnp.asarray(np.concatenate([inverse, inverse])[None, :])
     sends = 4 * (side - 1) + 2 * (side - 1) ** 2
-    anywhere = pl.BlockSpec(memory_space=pl.ANY)
+    anywhere = pl.BlockSpec(memory_space=pltpu.HBM)
     vmem = pl.BlockSpec(memory_space=pltpu.VMEM)
-    rows = tokens // CHUNKS
+    held = [
+        pltpu.with_memory_space_constraint(part, pltpu.HBM)
+        for part in (
+            decay_exponent, inverse, query_new, key_new, value_new, norm_gain.reshape(1, -1),
+            layer_input, key_weight, value_weight,
+        )
+    ]
     state_cache, first_read = pl.pallas_call(
         functools.partial(gather_kernel, side, seq_span, CHUNKS),
         out_shape=(
@@ -366,8 +417,8 @@
             pltpu.VMEM(value_weight.shape, BF16),
             pltpu.VMEM((tokens, width), F32),
             pltpu.VMEM((tokens, width), F32),
-            pltpu.VMEM((rows, heads * width), F32),
-            pltpu.VMEM((rows, heads * vwidth), F32),
+            pltpu.VMEM((tokens, heads * width), F32),
+            pltpu.VMEM((tokens, heads * vwidth), F32),
             pltpu.VMEM((heads, width, vwidth), F32),
             pltpu.VMEM((heads, width, vwidth), F32),
             pltpu.VMEM((SEQS, heads, 1, vwidth), F32),
@@ -383,14 +434,12 @@
             pltpu.SemaphoreType.DMA((groups, sp_size)),
             pltpu.SemaphoreType.DMA((sp_size - 1,)),
             pltpu.SemaphoreType.DMA((sp_size,)),
+            pltpu.SemaphoreType.REGULAR,
         ],
         compiler_params=pltpu.CompilerParams(
-            collective_id=0, has_side_effects=True, vmem_limit_bytes=62 * 1024 * 1024
+            collective_id=0, has_side_effects=True, vmem_limit_bytes=VMEM_KIB * 1024
         ),
-    )(
-        decay_exponent, inverse, query_new, key_new, value_new, norm_gain.reshape(1, -1),
-        layer_input, key_weight, value_weight,
-    )
+    )(*held)
     return pl.pallas_call(
         settle,
         out_shape=(
@@ -399,6 +448,7 @@
         ),
         in_specs=[vmem, vmem],
         out_specs=(vmem, vmem),
+        compiler_params=pltpu.CompilerParams(vmem_limit_bytes=4 * 1024 * 1024),
     )(state_cache, first_read)
 
 

time: 89.7 us -> 84.1 us (0.938)
  Pallas kernels: 88.9 us -> 83.3 us
    pallas_call x1, Pallas kernels: 87.4 us -> 82.7 us  [on_device(): pl.pallas_call(functools.partial(gather_kernel, side, seq_span, CHUNKS),...]
where the time goes in v1:
time: 84.1 us; the launch traced here: 83.9 us
  Pallas kernels  83.3 us (99%)
    pallas_call x1, Pallas kernels, on_device(): pl.pallas_call(functools.partial(gather_kernel, side, seq_span, CHUNKS),...  82.7 us

profile of v1, /device:TPU:0, one launch (start us, length us, event | category | flops | bytes accessed | tf_op | source)
XLA Modules:
  0.0 83.9 jit_solution(8101759314545651665)
XLA Ops:
  0.6 82.7 %shard_map.104 = (bf16[2,8,16,128]{3,2,1,0:T(8,128)(2,1)S(1)}, bf16[2,1024]{1,0:T(2,128)(2,1)S(1)}) custom-call(f32[8]{0:T(128)} %decay_hbm.1, f32[1,128]{1,0:T(1,128)} %constant.2.clone.inv_hbm, bf16[2,1024]{1,0:T(2,128)(2,1)} %query_hbm.1, bf16[2,1024]{1,0:T(2,128)(2,1)} %key_hbm.1, bf16[2,1024]{1,0:T(2,128)(2,1)} %value_hbm.1, f32[1,1024]{1,0:T(1,128)} %bitcast.1, ...), custom_call_target="tpu_custom_call" | custom-call | tf_op jit(solution)/shard_map/pallas_call | solution.py:400
  83.3 0.6 shard_map.105

commit v2 on v1

--- a/solution.py
+++ b/solution.py
@@ -22,10 +22,10 @@
     side, seq_span, chunks,
     decay_hbm, inv_hbm, query_hbm, key_hbm, value_hbm, gain_hbm, x_ref, wk_ref, wv_ref,
     cache_ref, first_ref,
-    decay_ref, inv_ref, query_ref, key_ref, value_ref, gain_ref,
-    gx, wk, wv, cosine, sine, acc_k, acc_v,
+    decay_ref, inv_ref, fresh_ref, gain_ref,
+    gx, w_ref, cosine, sine, acc_k, acc_v,
     state_ref, query_wide, own_term, factor, staged, landed, read, reads,
-    send_sem, recv_sem, local_sem, state_send, state_recv, read_send, read_recv, go_sem,
+    send_sem, recv_sem, local_sem, out_sem, go_sem, ready_sem,
 ):
     tokens, feats = x_ref.shape
     rows = tokens // chunks
@@ -58,25 +58,42 @@
     x_peers = [x_peer(d) for d in range(1, side)]
     y_peers = [y_peer(d) for d in range(1, side)]
 
-    fetch = pltpu.make_async_copy(x_ref, gx.at[me], local_sem.at[0])
-    fetch.start()
+    def fetch(first):
+        at = pl.ds(0, rows) if first else pl.ds(rows, tokens - rows)
+        return pltpu.make_async_copy(x_ref.at[at], gx.at[me, at], local_sem.at[0 if first else 1])
+
+    fetch(True).start()
+    mate = sp_place + 1 - 2 * core
     barrier = pltpu.get_barrier_semaphore()
     for peer in x_peers + y_peers:
         pl.semaphore_signal(barrier, inc=1, device_id={"tp": peer}, device_id_type=MESH)
-    for peer in sp_peers:
+    pl.semaphore_signal(barrier, inc=1, device_id={"sp": mate}, device_id_type=MESH)
+
+    def greet(peer, _):
         pl.semaphore_signal(barrier, inc=1, device_id={"sp": peer}, device_id_type=MESH)
-    pl.semaphore_wait(barrier, 2 * (side - 1) + sp_size - 1)
+        return 0
+
+    above = sp_place - core + 2
+    lax.fori_loop(above, sp_size, greet, 0)
+
+    if chunks > 1:
+        fetch(False).start()
+    pl.semaphore_wait(barrier, 2 * (side - 1) + 1 + sp_place - core)
+
+    def answer(peer, _):
+        pl.semaphore_signal(ready_sem, inc=1, device_id={"sp": peer}, device_id_type=MESH)
+        return 0
 
     def span(c, part):
         return pl.ds(pl.multiple_of(c * rows + part * half, half), half)
 
-    def remote(c, slot, block, part, target):
+    def remote(c, slot, block, part, target, kind):
         where = span(c, part)
         return pltpu.make_async_remote_copy(
             src_ref=gx.at[block, where],
             dst_ref=gx.at[block, where],
-            send_sem=send_sem.at[c, slot],
-            recv_sem=recv_sem.at[c, block, part],
+            send_sem=send_sem.at[slot],
+            recv_sem=recv_sem.at[kind, c],
             device_id={"tp": target},
             device_id_type=MESH,
         )
@@ -84,24 +101,25 @@
     fan = 2 * (side - 1)
 
     def own_copies(c, wave):
-        out, slot = [], wave * fan
+        out, slot = [], 0
         for peers, part in ((x_peers, wave), (y_peers, 1 - wave)):
             for peer in peers:
-                out.append(remote(c, slot, me, part, peer))
+                out.append(remote(c, slot, me, part, peer, wave))
                 slot += 1
         return out
 
     def relay_copies(c):
-        out, slot = [], 2 * fan
+        out, slot = [], fan
         for part, sources, peers in ((0, x_peers, y_peers), (1, y_peers, x_peers)):
-            for source in sources:
-                for peer in peers:
-                    out.append(remote(c, slot, source, part, peer))
-                    slot += 1
+            for peer in peers:
+                for source in sources:
+                    out.append(remote(c, slot, source, part, peer, 2))
+                slot += 1
         return out
 
-    def arrived(c, block, part):
-        remote(c, 0, block, part, x_peers[0]).wait_recv()
+    def arrived(c, kind, count):
+        spot = gx.at[pl.ds(0, count), pl.ds(0, rows)]
+        pltpu.make_async_copy(spot, spot, recv_sem.at[kind, c]).wait()
 
     late_blocks = [
         lax.rem(my_y + dy, side) * side + lax.rem(my_x + dx, side)
@@ -110,25 +128,24 @@
     ]
 
     def wait_wave(c, wave):
-        for block in x_peers:
-            arrived(c, block, wave)
-        for block in y_peers:
-            arrived(c, block, 1 - wave)
+        arrived(c, wave, side - 1)
 
     def wait_late(c):
-        for block in late_blocks:
-            for part in range(2):
-                arrived(c, block, part)
+        arrived(c, 2, (side - 1) ** 2)
 
     def start_all(copies):
         for copy in copies:
             copy.start()
 
-    def drain(copies):
-        for copy in copies:
-            copy.wait_send()
-
-    fetch.wait()
+    def drain_own():
+        for slot in range(fan):
+            pltpu.make_async_copy(gx.at[0], gx.at[0], send_sem.at[slot]).wait()
+
+    def drain_relay():
+        half_block = pl.ds(0, tokens // 2)
+        for slot in range(fan):
+            blocks = gx.at[pl.ds(0, side - 1), half_block]
+            pltpu.make_async_copy(blocks, blocks, send_sem.at[fan + slot]).wait()
 
     @pl.when(core == 1)
     def _():
@@ -139,26 +156,33 @@
             start_all(own_copies(c, wave))
             return 0
 
-        lax.fori_loop(0, chunks, body, 0)
-
+        lax.fori_loop(1 if wave == 0 else 0, chunks, body, 0)
+
+    fetch(True).wait()
+    start_all(own_copies(0, 0))
+    if chunks > 1:
+        fetch(False).wait()
     send_wave(0)
     send_wave(1)
+    lax.fori_loop(0, sp_place - core, answer, 0)
 
     small = [
-        pltpu.make_async_copy(source, target, local_sem.at[3 + i])
+        pltpu.make_async_copy(source, target, local_sem.at[2 + i])
         for i, (source, target) in enumerate((
-            (decay_hbm, decay_ref), (inv_hbm, inv_ref), (query_hbm, query_ref),
-            (key_hbm, key_ref), (value_hbm, value_ref), (gain_hbm, gain_ref),
+            (decay_hbm, decay_ref), (inv_hbm, inv_ref), (gain_hbm, gain_ref),
         ))
     ]
-    for copy in small:
-        copy.start()
-    local = [
-        pltpu.make_async_copy(wk_ref, wk, local_sem.at[1]),
-        pltpu.make_async_copy(wv_ref, wv, local_sem.at[2]),
+    fresh = [
+        pltpu.make_async_copy(source, fresh_ref.at[i], local_sem.at[5])
+        for i, source in enumerate((query_hbm, key_hbm, value_hbm))
     ]
-    for copy in local:
-        copy.start()
+    weights = [
+        pltpu.make_async_copy(source, w_ref.at[i], local_sem.at[6])
+        for i, source in enumerate((wk_ref, wv_ref))
+    ]
+    start_all(small)
+    start_all(fresh)
+    start_all(weights)
     state_ref[...] = jnp.zeros_like(state_ref)
 
     def pass_on(c):
@@ -178,6 +202,7 @@
 
     for copy in small:
         copy.wait()
+    pltpu.make_async_copy(fresh_ref, fresh_ref, local_sem.at[5]).wait()
     base = lax.rem(sp_place, seq_span) * tokens
 
     def table(c, _):
@@ -197,9 +222,7 @@
         jnp.int32, (width, width), 1
     )
     ones = jnp.ones((width, vwidth), BF16)
-    queries = query_ref[...].astype(F32)
-    next_keys = key_ref[...].astype(F32)
-    next_values = value_ref[...].astype(F32)
+    queries, next_keys, next_values = (fresh_ref[i].astype(F32) for i in range(3))
     for h in range(heads):
         cols = slice(h * width, (h + 1) * width)
         vcols = slice(h * vwidth, (h + 1) * vwidth)
@@ -220,29 +243,35 @@
             pltpu.make_async_remote_copy(
                 src_ref=staged.at[peer, piece],
                 dst_ref=landed.at[sp_place, piece],
-                send_sem=state_send.at[g, d],
-                recv_sem=state_recv.at[g, sp_place],
+                send_sem=out_sem.at[0],
+                recv_sem=out_sem.at[1],
                 device_id={"sp": peer},
                 device_id_type=MESH,
             )
-            for d, peer in enumerate(sp_peers)
+            for peer in sp_peers
         ]
 
-    def read_copies():
+    def read_copies(g):
+        piece = pl.ds(g * pair, pair)
         return [
             pltpu.make_async_remote_copy(
-                src_ref=read,
-                dst_ref=reads.at[sp_place],
-                send_sem=read_send.at[d],
-                recv_sem=read_recv.at[sp_place],
+                src_ref=read.at[piece],
+                dst_ref=reads.at[sp_place, piece],
+                send_sem=out_sem.at[2],
+                recv_sem=out_sem.at[3],
                 device_id={"sp": peer},
                 device_id_type=MESH,
             )
-            for d, peer in enumerate(sp_peers)
+            for peer in sp_peers
         ]
 
-    for copy in local:
-        copy.wait()
+    def hand_out(g):
+        for state_copy, read_copy in zip(state_copies(g), read_copies(g)):
+            read_copy.start()
+            state_copy.start()
+
+    pltpu.make_async_copy(w_ref, w_ref, local_sem.at[6]).wait()
+    wk, wv = w_ref.at[0], w_ref.at[1]
 
     def partial(c, blocks, w, cols):
         at = pl.ds(pl.multiple_of(c * rows, rows), rows)
@@ -299,51 +328,36 @@
                     for d in range(sp_size):
                         staged[d, h] = held[d * kept:(d + 1) * kept, :].astype(BF16)
                     read[h] = jnp.sum(query_wide[h] * held, axis=0, keepdims=True)
-                start_all(state_copies(g))
+                hand_out(g)
             return 0
 
         lax.fori_loop(0, groups, step, 0)
 
     def finish_loop(c, _):
         finish(c, False)
-        return 0
-
-    def drain_wave(wave):
-        def body(c, _):
-            drain(own_copies(c, wave))
-            return 0
-
-        lax.fori_loop(0, chunks, body, 0)
-
-    def drain_relay(c, _):
-        drain(relay_copies(c))
         return 0
 
     lax.fori_loop(lead, chunks, pass_on_loop, 0)
     lax.fori_loop(0, chunks, early, 0)
     lax.fori_loop(0, chunks - 1, finish_loop, 0)
-    drain_wave(0)
-    drain_wave(1)
+    drain_own()
+
+    @pl.when(above < sp_size)
+    def _():
+        pl.semaphore_wait(ready_sem, sp_size - above)
+
     finish(chunks - 1, True)
 
-    start_all(read_copies())
     landed[sp_place] = staged[sp_place]
     reads[sp_place] = read[...]
-    lax.fori_loop(0, chunks, drain_relay, 0)
-
-    for d, peer in enumerate(sp_peers):
-        pltpu.make_async_remote_copy(
-            src_ref=read, dst_ref=reads.at[peer], send_sem=read_send.at[d],
-            recv_sem=read_recv.at[peer], device_id={"sp": peer}, device_id_type=MESH,
-        ).wait_recv()
-        for g in range(groups):
-            piece = pl.ds(g * pair, pair)
-            pltpu.make_async_remote_copy(
-                src_ref=staged.at[peer, piece], dst_ref=landed.at[peer, piece],
-                send_sem=state_send.at[g, d], recv_sem=state_recv.at[g, peer],
-                device_id={"sp": peer}, device_id_type=MESH,
-            ).wait_recv()
-
+    drain_relay()
+
+    def exchanged(which):
+        others = pl.ds(0, sp_size - 1)
+        pltpu.make_async_copy(staged.at[others], landed.at[others], out_sem.at[which]).wait()
+        pltpu.make_async_copy(reads.at[others], reads.at[others], out_sem.at[2 + which]).wait()
+
+    exchanged(1)
     row = lax.broadcasted_iota(jnp.int32, (SEQS, heads * vwidth), 0)
     out = jnp.zeros((SEQS, heads * vwidth), F32)
     for s in range(SEQS):
@@ -359,11 +373,7 @@
             ).astype(BF16)
     first_ref[...] = out.astype(BF16)
 
-    for copy in read_copies():
-        copy.wait_send()
-    for g in range(groups):
-        for copy in state_copies(g):
-            copy.wait_send()
+    exchanged(0)
 
 
 def settle(cache_ref, first_ref, cache_out, first_out):
@@ -383,11 +393,9 @@
     width = key_weight.shape[1] // heads
     vwidth = value_weight.shape[1] // heads
     kept = width // sp_size
-    groups = heads // next(p for p in (4, 2, 1) if heads % p == 0)
     steps = np.linspace(0.0, 1.0, width // 2, dtype=np.float32)
     inverse = (np.float32(1.0) / np.power(np.float32(10000.0), steps)).astype(np.float32)
     inverse = jnp.asarray(np.concatenate([inverse, inverse])[None, :])
-    sends = 4 * (side - 1) + 2 * (side - 1) ** 2
     anywhere = pl.BlockSpec(memory_space=pltpu.HBM)
     vmem = pl.BlockSpec(memory_space=pltpu.VMEM)
     held = [
@@ -408,13 +416,10 @@
         scratch_shapes=[
             pltpu.SMEM((heads,), F32),
             pltpu.VMEM(inverse.shape, F32),
-            pltpu.VMEM(query_new.shape, BF16),
-            pltpu.VMEM(key_new.shape, BF16),
-            pltpu.VMEM(value_new.shape, BF16),
+            pltpu.VMEM((3,) + query_new.shape, BF16),
             pltpu.VMEM((1, heads * vwidth), F32),
             pltpu.VMEM((parts, tokens, feats), BF16),
-            pltpu.VMEM(key_weight.shape, BF16),
-            pltpu.VMEM(value_weight.shape, BF16),
+            pltpu.VMEM((2,) + key_weight.shape, BF16),
             pltpu.VMEM((tokens, width), F32),
             pltpu.VMEM((tokens, width), F32),
             pltpu.VMEM((tokens, heads * width), F32),
@@ -427,13 +432,11 @@
             pltpu.VMEM((sp_size, heads, kept, vwidth), BF16),
             pltpu.VMEM((heads, 1, vwidth), F32),
             pltpu.VMEM((sp_size, heads, 1, vwidth), F32),
-            pltpu.SemaphoreType.DMA((CHUNKS, sends)),
-            pltpu.SemaphoreType.DMA((CHUNKS, parts, 2)),
-            pltpu.SemaphoreType.DMA((9,)),
-            pltpu.SemaphoreType.DMA((groups, sp_size - 1)),
-            pltpu.SemaphoreType.DMA((groups, sp_size)),
-            pltpu.SemaphoreType.DMA((sp_size - 1,)),
-            pltpu.SemaphoreType.DMA((sp_size,)),
+            pltpu.SemaphoreType.DMA((4 * (side - 1),)),
+            pltpu.SemaphoreType.DMA((3, CHUNKS)),
+            pltpu.SemaphoreType.DMA((7,)),
+            pltpu.SemaphoreType.DMA((4,)),
+            pltpu.SemaphoreType.REGULAR,
             pltpu.SemaphoreType.REGULAR,
         ],
         compiler_params=pltpu.CompilerParams(

time: 84.1 us -> 82.2 us (0.977)
  Pallas kernels: 83.3 us -> 81.3 us
    pallas_call x1, Pallas kernels: 82.7 us -> 80.6 us  [on_device(): pl.pallas_call(functools.partial(gather_kernel, side, seq_span, CHUNKS),...]
where the time goes in v2:
time: 82.2 us; the launch traced here: 81.9 us
  Pallas kernels  81.3 us (99%)
    pallas_call x1, Pallas kernels, on_device(): pl.pallas_call(functools.partial(gather_kernel, side, seq_span, CHUNKS),...  80.6 us

profile of v2, /device:TPU:0, one launch (start us, length us, event | category | flops | bytes accessed | tf_op | source)
XLA Modules:
  0.0 81.9 jit_solution(11686218704677682529)
XLA Ops:
  0.6 80.6 %shard_map.104 = (bf16[2,8,16,128]{3,2,1,0:T(8,128)(2,1)S(1)}, bf16[2,1024]{1,0:T(2,128)(2,1)S(1)}) custom-call(f32[8]{0:T(128)} %decay_hbm.1, f32[1,128]{1,0:T(1,128)} %constant.2.clone.inv_hbm, bf16[2,1024]{1,0:T(2,128)(2,1)} %query_hbm.1, bf16[2,1024]{1,0:T(2,128)(2,1)} %key_hbm.1, bf16[2,1024]{1,0:T(2,128)(2,1)} %value_hbm.1, f32[1,1024]{1,0:T(1,128)} %bitcast.1, ...), custom_call_target="tpu_custom_call" | custom-call | tf_op jit(solution)/shard_map/pallas_call | solution.py:408
  81.3 0.6 shard_map.105

commit v3 on v2

--- a/solution.py
+++ b/solution.py
@@ -12,6 +12,7 @@
 SEQS = 2
 CHUNKS = 8
 LEAD = 1
+CUTS = 1
 VMEM_KIB = 48 * 1024
 MESH = pl.DeviceIdType.MESH
 F32 = jnp.float32
@@ -24,8 +25,8 @@
     cache_ref, first_ref,
     decay_ref, inv_ref, fresh_ref, gain_ref,
     gx, w_ref, cosine, sine, acc_k, acc_v,
-    state_ref, query_wide, own_term, factor, staged, landed, read, reads,
-    send_sem, recv_sem, local_sem, out_sem, go_sem, ready_sem,
+    state_ref, fade, shrink, query_wide, own_term, factor, staged, landed, read, reads,
+    send_sem, recv_sem, local_sem, out_sem, go_sem, ready_sem, x_sem, y_sem, mate_sem,
 ):
     tokens, feats = x_ref.shape
     rows = tokens // chunks
@@ -63,62 +64,87 @@
         return pltpu.make_async_copy(x_ref.at[at], gx.at[me, at], local_sem.at[0 if first else 1])
 
     fetch(True).start()
-    mate = sp_place + 1 - 2 * core
     barrier = pltpu.get_barrier_semaphore()
+    below = sp_place - core
+    above = below + 2
+
+    def tell(semaphore, axis, peer):
+        pl.semaphore_signal(semaphore, inc=1, device_id={axis: peer}, device_id_type=MESH)
+
+    def expect(semaphore, count):
+        @pl.when(count > 0)
+        def _():
+            pl.semaphore_wait(semaphore, count)
+
     for peer in x_peers + y_peers:
-        pl.semaphore_signal(barrier, inc=1, device_id={"tp": peer}, device_id_type=MESH)
-    pl.semaphore_signal(barrier, inc=1, device_id={"sp": mate}, device_id_type=MESH)
+        pl.when(peer > me)(functools.partial(tell, barrier, "tp", peer))
+
+    @pl.when(core == 0)
+    def _():
+        tell(barrier, "sp", sp_place + 1)
 
     def greet(peer, _):
-        pl.semaphore_signal(barrier, inc=1, device_id={"sp": peer}, device_id_type=MESH)
-        return 0
-
-    above = sp_place - core + 2
+        tell(barrier, "sp", peer)
+        return 0
+
     lax.fori_loop(above, sp_size, greet, 0)
-
+    expect(barrier, my_x + my_y + sp_place)
+    for peer in x_peers:
+        pl.when(peer < me)(functools.partial(tell, x_sem, "tp", peer))
+    for peer in y_peers:
+        pl.when(peer < me)(functools.partial(tell, y_sem, "tp", peer))
+
+    @pl.when(core == 1)
+    def _():
+        tell(mate_sem, "sp", sp_place - 1)
+
+    fetch(True).wait()
     if chunks > 1:
         fetch(False).start()
-    pl.semaphore_wait(barrier, 2 * (side - 1) + 1 + sp_place - core)
 
     def answer(peer, _):
-        pl.semaphore_signal(ready_sem, inc=1, device_id={"sp": peer}, device_id_type=MESH)
+        tell(ready_sem, "sp", peer)
         return 0
 
     def span(c, part):
         return pl.ds(pl.multiple_of(c * rows + part * half, half), half)
 
-    def remote(c, slot, block, part, target, kind):
-        where = span(c, part)
+    def remote(c, slot, block, part, target, kind, cut=None):
+        where = (block, span(c, part))
+        if cut is not None:
+            where += (pl.ds(cut * (feats // CUTS), feats // CUTS),)
         return pltpu.make_async_remote_copy(
-            src_ref=gx.at[block, where],
-            dst_ref=gx.at[block, where],
+            src_ref=gx.at[where],
+            dst_ref=gx.at[where],
             send_sem=send_sem.at[slot],
-            recv_sem=recv_sem.at[kind, c],
+            recv_sem=recv_sem.at[kind, c + (cut or 0)],
             device_id={"tp": target},
             device_id_type=MESH,
         )
 
     fan = 2 * (side - 1)
 
-    def own_copies(c, wave):
-        out, slot = [], 0
-        for peers, part in ((x_peers, wave), (y_peers, 1 - wave)):
-            for peer in peers:
-                out.append(remote(c, slot, me, part, peer, wave))
-                slot += 1
+    def own_copies(c, wave, along_x):
+        out, slot = [], 0 if along_x else side - 1
+        for peer in x_peers if along_x else y_peers:
+            part = wave if along_x else 1 - wave
+            out.append(remote(c, slot, me, part, peer, wave))
+            slot += 1
         return out
 
-    def relay_copies(c):
-        out, slot = [], fan
-        for part, sources, peers in ((0, x_peers, y_peers), (1, y_peers, x_peers)):
-            for peer in peers:
-                for source in sources:
-                    out.append(remote(c, slot, source, part, peer, 2))
-                slot += 1
+    def relay_copies(c, cuts=(None,)):
+        out = []
+        for cut in cuts:
+            slot = fan
+            for part, sources, peers in ((0, x_peers, y_peers), (1, y_peers, x_peers)):
+                for peer in peers:
+                    for source in sources:
+                        out.append(remote(c, slot, source, part, peer, 2, cut))
+                    slot += 1
         return out
 
-    def arrived(c, kind, count):
-        spot = gx.at[pl.ds(0, count), pl.ds(0, rows)]
+    def arrived(c, kind, count, cuts=1):
+        spot = gx.at[pl.ds(0, count), pl.ds(0, rows), pl.ds(0, feats // cuts)]
         pltpu.make_async_copy(spot, spot, recv_sem.at[kind, c]).wait()
 
     late_blocks = [
@@ -130,8 +156,8 @@
     def wait_wave(c, wave):
         arrived(c, wave, side - 1)
 
-    def wait_late(c):
-        arrived(c, 2, (side - 1) ** 2)
+    def wait_late(c, cuts=1):
+        arrived(c, 2, (side - 1) ** 2, cuts)
 
     def start_all(copies):
         for copy in copies:
@@ -147,24 +173,41 @@
             blocks = gx.at[pl.ds(0, side - 1), half_block]
             pltpu.make_async_copy(blocks, blocks, send_sem.at[fan + slot]).wait()
 
+
     @pl.when(core == 1)
     def _():
         pl.semaphore_wait(go_sem, 1)
 
+    def send_first(along_x):
+        start_all(own_copies(0, 0, along_x))
+
+    x_last, y_last = my_x == side - 1, my_y == side - 1
+    pl.when(x_last)(functools.partial(send_first, True))
+    pl.when(y_last)(functools.partial(send_first, False))
+
+    @pl.when(jnp.logical_not(x_last))
+    def _():
+        expect(x_sem, side - 1 - my_x)
+        send_first(True)
+
+    @pl.when(jnp.logical_not(y_last))
+    def _():
+        expect(y_sem, side - 1 - my_y)
+        send_first(False)
+
+    if chunks > 1:
+        fetch(False).wait()
+
     def send_wave(wave):
         def body(c, _):
-            start_all(own_copies(c, wave))
+            start_all(own_copies(c, wave, True) + own_copies(c, wave, False))
             return 0
 
-        lax.fori_loop(1 if wave == 0 else 0, chunks, body, 0)
-
-    fetch(True).wait()
-    start_all(own_copies(0, 0))
-    if chunks > 1:
-        fetch(False).wait()
+        lax.fori_loop(1 - wave, chunks, body, 0)
+
     send_wave(0)
     send_wave(1)
-    lax.fori_loop(0, sp_place - core, answer, 0)
+    lax.fori_loop(0, below, answer, 0)
 
     small = [
         pltpu.make_async_copy(source, target, local_sem.at[2 + i])
@@ -185,37 +228,51 @@
     start_all(weights)
     state_ref[...] = jnp.zeros_like(state_ref)
 
-    def pass_on(c):
+    def pass_on(c, cuts=(None,)):
         wait_wave(c, 0)
-        start_all(relay_copies(c))
+        start_all(relay_copies(c, cuts))
 
     def pass_on_loop(c, _):
         pass_on(c)
         return 0
 
-    lead = min(LEAD, chunks)
+    lead, last = min(LEAD, chunks - 1), chunks - 1
     lax.fori_loop(0, lead, pass_on_loop, 0)
 
     @pl.when(core == 0)
     def _():
-        pl.semaphore_signal(go_sem, inc=1, device_id={"sp": sp_place + 1}, device_id_type=MESH)
+        pl.semaphore_wait(mate_sem, 1)
+        tell(go_sem, "sp", sp_place + 1)
 
     for copy in small:
         copy.wait()
     pltpu.make_async_copy(fresh_ref, fresh_ref, local_sem.at[5]).wait()
     base = lax.rem(sp_place, seq_span) * tokens
+
+    scale = width ** (-0.5)
 
     def table(c, _):
         at = pl.ds(pl.multiple_of(c * half, half), half)
         place = (base + c * half + lax.broadcasted_iota(jnp.int32, (half, width), 0)).astype(F32)
         angle = place * inv_ref[...]
         low = lax.broadcasted_iota(jnp.int32, (half, width), 1) < width // 2
-        sin = jnp.sin(angle)
-        cosine[at, :] = jnp.cos(angle)
+        sin = jnp.sin(angle) * scale
+        cosine[at, :] = jnp.cos(angle) * scale
         sine[at, :] = jnp.where(low, -sin, sin)
         return 0
 
     lax.fori_loop(0, 2 * chunks, table, 0)
+    distance = (seq_span * tokens - tokens - base + rows - 1) - lax.broadcasted_iota(
+        jnp.int32, (rows, width), 0
+    )
+    distance = distance.astype(F32)
+
+    def fading(h, _):
+        fade[h] = jnp.exp(decay_ref[h] * distance)
+        shrink[h] = jnp.exp(jnp.full((1, vwidth), decay_ref[h] * rows, F32))
+        return 0
+
+    lax.fori_loop(0, heads, fading, 0)
 
     prompt = sp_place // seq_span
     diagonal = lax.broadcasted_iota(jnp.int32, (width, width), 0) == lax.broadcasted_iota(
@@ -273,12 +330,16 @@
     pltpu.make_async_copy(w_ref, w_ref, local_sem.at[6]).wait()
     wk, wv = w_ref.at[0], w_ref.at[1]
 
-    def partial(c, blocks, w, cols):
+    def partial(c, blocks, w, cols, cut=0, cuts=1):
         at = pl.ds(pl.multiple_of(c * rows, rows), rows)
+        deep = feats // cuts
         total = None
         for block in blocks:
-            depth = pl.ds(pl.multiple_of(block * feats, feats), feats)
-            term = jnp.dot(gx[block, at, :], w[depth, cols], preferred_element_type=F32)
+            depth = pl.ds(pl.multiple_of(block * feats + cut * deep, deep), deep)
+            term = jnp.dot(
+                gx[block, at, pl.ds(cut * deep, deep)], w[depth, cols],
+                preferred_element_type=F32,
+            )
             total = term if total is None else total + term
         return total
 
@@ -298,36 +359,54 @@
         lax.fori_loop(0, groups, step, 0)
         return 0
 
+    def columns(g):
+        return (
+            pl.ds(pl.multiple_of(g * pair * width, pair * width), pair * width),
+            pl.ds(pl.multiple_of(g * pair * vwidth, pair * vwidth), pair * vwidth),
+        )
+
+    def head_start(c, cut):
+        wait_late(c + cut, CUTS)
+        at = pl.ds(pl.multiple_of(c * rows, rows), rows)
+
+        def step(g, _):
+            kcols, vcols = columns(g)
+            acc_k[at, kcols] += partial(c, late_blocks, wk, kcols, cut, CUTS)
+            acc_v[at, vcols] += partial(c, late_blocks, wv, vcols, cut, CUTS)
+            return 0
+
+        lax.fori_loop(0, groups, step, 0)
+
     def finish(c, last):
-        wait_late(c)
+        if last:
+            for cut in range(CUTS - 1):
+                head_start(c, cut)
+            wait_late(c + CUTS - 1, CUTS)
+        else:
+            wait_late(c)
         at = pl.ds(pl.multiple_of(c * rows, rows), rows)
-        distance = (seq_span * tokens - 1 - base - c * rows) - lax.broadcasted_iota(
-            jnp.int32, (rows, width), 0
-        )
-        distance = distance.astype(F32)
+        cut = (CUTS - 1, CUTS) if last else (0, 1)
 
         def step(g, _):
-            kcols = pl.ds(pl.multiple_of(g * pair * width, pair * width), pair * width)
-            vcols = pl.ds(pl.multiple_of(g * pair * vwidth, pair * vwidth), pair * vwidth)
-            k = partial(c, late_blocks, wk, kcols) + acc_k[at, kcols]
-            v = partial(c, late_blocks, wv, vcols) + acc_v[at, vcols]
+            kcols, vcols = columns(g)
+            k = partial(c, late_blocks, wk, kcols, *cut) + acc_k[at, kcols]
+            v = partial(c, late_blocks, wv, vcols, *cut) + acc_v[at, vcols]
             v = v.astype(BF16)
             for j in range(pair):
+                h = g * pair + j
                 kh = k[:, j * width:(j + 1) * width]
                 turned = kh * cosine[at, :] + pltpu.roll(kh, width // 2, 1) * sine[at, :]
-                keys = (turned * width ** (-0.5)).astype(BF16).astype(F32)
-                weighted = (keys * jnp.exp(decay_ref[g * pair + j] * distance)).astype(BF16)
-                state_ref[g * pair + j] += lax.dot_general(
-                    weighted, v[:, j * vwidth:(j + 1) * vwidth],
+                held = state_ref[h] * shrink[h] + lax.dot_general(
+                    (turned * fade[h]).astype(BF16), v[:, j * vwidth:(j + 1) * vwidth],
                     (((0,), (0,)), ((), ())), preferred_element_type=F32,
                 )
-            if last:
-                for j in range(pair):
-                    h = g * pair + j
-                    held = state_ref[h]
+                if last:
                     for d in range(sp_size):
                         staged[d, h] = held[d * kept:(d + 1) * kept, :].astype(BF16)
                     read[h] = jnp.sum(query_wide[h] * held, axis=0, keepdims=True)
+                else:
+                    state_ref[h] = held
+            if last:
                 hand_out(g)
             return 0
 
@@ -337,14 +416,13 @@
         finish(c, False)
         return 0
 
-    lax.fori_loop(lead, chunks, pass_on_loop, 0)
+    lax.fori_loop(lead, last, pass_on_loop, 0)
+    pass_on(last, range(CUTS))
     lax.fori_loop(0, chunks, early, 0)
     lax.fori_loop(0, chunks - 1, finish_loop, 0)
     drain_own()
 
-    @pl.when(above < sp_size)
-    def _():
-        pl.semaphore_wait(ready_sem, sp_size - above)
+    expect(ready_sem, sp_size - above)
 
     finish(chunks - 1, True)
 
@@ -425,6 +503,8 @@
             pltpu.VMEM((tokens, heads * width), F32),
             pltpu.VMEM((tokens, heads * vwidth), F32),
             pltpu.VMEM((heads, width, vwidth), F32),
+            pltpu.VMEM((heads, tokens // CHUNKS, width), F32),
+            pltpu.VMEM((heads, 1, vwidth), F32),
             pltpu.VMEM((heads, width, vwidth), F32),
             pltpu.VMEM((SEQS, heads, 1, vwidth), F32),
             pltpu.VMEM((heads, 1, vwidth), F32),
@@ -433,9 +513,12 @@
             pltpu.VMEM((heads, 1, vwidth), F32),
             pltpu.VMEM((sp_size, heads, 1, vwidth), F32),
             pltpu.SemaphoreType.DMA((4 * (side - 1),)),
-            pltpu.SemaphoreType.DMA((3, CHUNKS)),
+            pltpu.SemaphoreType.DMA((3, CHUNKS + CUTS - 1)),
             pltpu.SemaphoreType.DMA((7,)),
             pltpu.SemaphoreType.DMA((4,)),
+            pltpu.SemaphoreType.REGULAR,
+            pltpu.SemaphoreType.REGULAR,
+            pltpu.SemaphoreType.REGULAR,
             pltpu.SemaphoreType.REGULAR,
             pltpu.SemaphoreType.REGULAR,
         ],

time: 82.2 us -> 81.7 us (level)
  no operation moved by 1% of the time
where the time goes in v3:
time: 81.7 us; the launch traced here: 81.4 us
  Pallas kernels  80.8 us (99%)
    pallas_call x1, Pallas kernels, on_device(): pl.pallas_call(functools.partial(gather_kernel, side, seq_span, CHUNKS),...  80.2 us

profile of v3, /device:TPU:0, one launch (start us, length us, event | category | flops | bytes accessed | tf_op | source)
XLA Modules:
  0.0 81.4 jit_solution(14091896216770947458)
XLA Ops:
  0.6 80.2 %shard_map.104 = (bf16[2,8,16,128]{3,2,1,0:T(8,128)(2,1)S(1)}, bf16[2,1024]{1,0:T(2,128)(2,1)S(1)}) custom-call(f32[8]{0:T(128)} %decay_hbm.1, f32[1,128]{1,0:T(1,128)} %constant.2.clone.inv_hbm, bf16[2,1024]{1,0:T(2,128)(2,1)} %query_hbm.1, bf16[2,1024]{1,0:T(2,128)(2,1)} %key_hbm.1, bf16[2,1024]{1,0:T(2,128)(2,1)} %value_hbm.1, f32[1,1024]{1,0:T(1,128)} %bitcast.1, ...), custom_call_target="tpu_custom_call" | custom-call | tf_op jit(solution)/shard_map/pallas_call | solution.py:486
  80.8 0.6 shard_map.105

commit v4 on v3

v4 whole, which is shorter than its diff:
```python
import functools
import math

import jax
import jax.numpy as jnp
import numpy as np
from jax import lax
from jax.experimental import pallas as pl
from jax.experimental.pallas import tpu as pltpu
from jax.sharding import PartitionSpec as P

SEQS = 2
CHUNKS = 8
LEAD = 1
SLIP = 16
VMEM_KIB = 48 * 1024
MESH = pl.DeviceIdType.MESH
F32 = jnp.float32
BF16 = jnp.bfloat16


def gather_kernel(
    side, seq_span, chunks,
    decay_hbm, inv_hbm, query_hbm, key_hbm, value_hbm, gain_hbm, x_ref, wk_ref, wv_ref,
    cache_ref, first_ref,
    decay_ref, inv_ref, fresh_ref, gain_ref,
    gx, w_ref, cosine, sine, acc_k, acc_v,
    state_ref, fade, shrink, query_wide, own_term, factor, staged, landed, read, reads,
    k_tmp, v_tmp, guest_fade, guest_wide, guest_staged, guest_landed, guest_read, guest_reads,
    send_sem, recv_sem, slip_send, slip_recv, local_sem, out_sem, guest_sem,
    go_sem, ready_sem, x_sem, y_sem, mate_sem,
):
    tokens, feats = x_ref.shape
    rows = tokens // chunks
    half = rows // 2
    slip = SLIP
    last = chunks - 1
    heads, width, vwidth = state_ref.shape
    pair = next(p for p in (4, 2, 1) if heads % p == 0)
    me = lax.axis_index("tp")
    my_y, my_x = me // side, lax.rem(me, side)
    sp_place = lax.axis_index("sp")
    sp_size = landed.shape[0]
    kept = landed.shape[2]
    groups = heads // pair
    core = lax.rem(sp_place, 2)
    shift = sp_size - 2
    donor, host = sp_place >= shift, sp_place < 2
    full = jnp.logical_not(donor)

    sp_peers = [jnp.where(sp_place > p, p, p + 1) for p in range(sp_size - 1)]

    def x_peer(d):
        return my_y * side + lax.rem(my_x + d, side)

    def y_peer(d):
        return lax.rem(my_y + d, side) * side + my_x

    x_peers = [x_peer(d) for d in range(1, side)]
    y_peers = [y_peer(d) for d in range(1, side)]
    late_blocks = [
        lax.rem(my_y + dy, side) * side + lax.rem(my_x + dx, side)
        for dy in range(1, side)
        for dx in range(1, side)
    ]
    early_blocks = [me] + x_peers + y_peers

    def fetch(first):
        at = pl.ds(0, rows) if first else pl.ds(rows, tokens - rows)
        return pltpu.make_async_copy(x_ref.at[at], gx.at[me, at], local_sem.at[0 if first else 1])

    fetch(True).start()
    barrier = pltpu.get_barrier_semaphore()
    below = sp_place - core
    above = below + 2

    def tell(semaphore, axis, peer):
        pl.semaphore_signal(semaphore, inc=1, device_id={axis: peer}, device_id_type=MESH)

    def expect(semaphore, count):
        @pl.when(count > 0)
        def _():
            pl.semaphore_wait(semaphore, count)

    for peer in x_peers + y_peers:
        pl.when(peer > me)(functools.partial(tell, barrier, "tp", peer))

    @pl.when(core == 0)
    def _():
        tell(barrier, "sp", sp_place + 1)

    def greet(peer, _):
        tell(barrier, "sp", peer)
        return 0

    lax.fori_loop(above, sp_size, greet, 0)
    expect(barrier, my_x + my_y + sp_place)
    for peer in x_peers:
        pl.when(peer < me)(functools.partial(tell, x_sem, "tp", peer))
    for peer in y_peers:
        pl.when(peer < me)(functools.partial(tell, y_sem, "tp", peer))

    @pl.when(core == 1)
    def _():
        tell(mate_sem, "sp", sp_place - 1)

    fetch(True).wait()
    fetch(False).start()

    def answer(peer, _):
        tell(ready_sem, "sp", peer)
        return 0

    def chunk_plot(c, count):
        return (
            lambda part: pl.multiple_of(c * rows + part * half, half),
            count, lambda slot: send_sem.at[slot], lambda kind: recv_sem.at[kind, c],
        )

    def slip_plot(which):
        return (
            lambda part: tokens + part * slip if which else last * rows + (part + 1) * half - slip,
            slip, lambda slot: slip_send.at[which], lambda kind: slip_recv.at[which, kind],
        )

    last_plot, tail_plot, guest_plot = chunk_plot(last, half - slip), slip_plot(0), slip_plot(1)

    def remote(plot, slot, block, part, target, kind):
        start, count, send, recv = plot
        where = (block, pl.ds(start(part), count))
        return pltpu.make_async_remote_copy(
            src_ref=gx.at[where],
            dst_ref=gx.at[where],
            send_sem=send(slot),
            recv_sem=recv(kind),
            device_id={"tp": target},
            device_id_type=MESH,
        )

    fan = 2 * (side - 1)

    def along(plot, wave, on_x):
        part = wave if on_x else 1 - wave
        first = 0 if on_x else side - 1
        return [
            remote(plot, first + slot, me, part, peer, wave)
            for slot, peer in enumerate(x_peers if on_x else y_peers)
        ]

    def own_copies(plot, wave):
        return along(plot, wave, True) + along(plot, wave, False)

    def relay_copies(plot):
        out, slot = [], fan
        for part, sources, peers in ((0, x_peers, y_peers), (1, y_peers, x_peers)):
            for peer in peers:
                for source in sources:
                    out.append(remote(plot, slot, source, part, peer, 2))
                slot += 1
        return out

    def arrived(plot, kind):
        blocks = (side - 1) ** 2 if kind == 2 else side - 1
        spot = gx.at[pl.ds(0, blocks), pl.ds(0, 2 * plot[1])]
        pltpu.make_async_copy(spot, spot, plot[3](kind)).wait()

    def start_all(copies):
        for copy in copies:
            copy.start()

    def settled(blocks, count, semaphore):
        spot = gx.at[pl.ds(0, blocks), pl.ds(0, count)]
        pltpu.make_async_copy(spot, spot, semaphore).wait()

    def lend():
        return [
            pltpu.make_async_remote_copy(
                src_ref=gx.at[me, pl.ds(tail_plot[0](part), slip)],
                dst_ref=gx.at[me, pl.ds(guest_plot[0](part), slip)],
                send_sem=guest_sem.at[0],
                recv_sem=guest_sem.at[1],
                device_id={"sp": sp_place - shift},
                device_id_type=MESH,
            )
            for part in range(2)
        ]

    @pl.when(core == 1)
    def _():
        pl.semaphore_wait(go_sem, 1)

    def send_first(on_x):
        start_all(along(chunk_plot(0, half), 0, on_x))

    x_last, y_last = my_x == side - 1, my_y == side - 1
    pl.when(x_last)(functools.partial(send_first, True))
    pl.when(y_last)(functools.partial(send_first, False))

    @pl.when(jnp.logical_not(x_last))
    def _():
        expect(x_sem, side - 1 - my_x)
        send_first(True)

    @pl.when(jnp.logical_not(y_last))
    def _():
        expect(y_sem, side - 1 - my_y)
        send_first(False)

    fetch(False).wait()

    @pl.when(donor)
    def _():
        start_all(lend())
        for block in x_peers + y_peers + late_blocks:
            for part in range(2):
                gx[block, pl.ds(tail_plot[0](part), slip), :] = jnp.zeros((slip, feats), BF16)

    def send_own(wave):
        def body(c, _):
            start_all(own_copies(chunk_plot(c, half), wave))
            return 0

        lax.fori_loop(1 - wave, last, body, 0)
        start_all(own_copies(last_plot, wave))

        @pl.when(full)
        def _():
            start_all(own_copies(tail_plot, wave))

    send_own(0)
    lax.fori_loop(0, below, answer, 0)

    small = [
        pltpu.make_async_copy(source, target, local_sem.at[2 + i])
        for i, (source, target) in enumerate((
            (decay_hbm, decay_ref), (inv_hbm, inv_ref), (gain_hbm, gain_ref),
        ))
    ]
    fresh = [
        pltpu.make_async_copy(source, fresh_ref.at[i], local_sem.at[5])
        for i, source in enumerate((query_hbm, key_hbm, value_hbm))
    ]
    weights = [
        pltpu.make_async_copy(source, w_ref.at[i], local_sem.at[6])
        for i, source in enumerate((wk_ref, wv_ref))
    ]
    start_all(small)
    start_all(fresh)
    start_all(weights)
    state_ref[...] = jnp.zeros_like(state_ref)

    def pass_on(plot):
        arrived(plot, 0)
        start_all(relay_copies(plot))

    def pass_on_loop(c, _):
        pass_on(chunk_plot(c, half))
        return 0

    lax.fori_loop(0, LEAD, pass_on_loop, 0)

    @pl.when(core == 0)
    def _():
        pl.semaphore_wait(mate_sem, 1)
        tell(go_sem, "sp", sp_place + 1)

    for copy in small:
        copy.wait()
    pltpu.make_async_copy(fresh_ref, fresh_ref, local_sem.at[5]).wait()
    base = lax.rem(sp_place, seq_span) * tokens
    guest_place = lax.rem(sp_place + shift, sp_size)
    guest_base = lax.rem(guest_place, seq_span) * tokens
    scale = width ** (-0.5)

    def fill(at, count, first):
        place = (first + lax.broadcasted_iota(jnp.int32, (count, width), 0)).astype(F32)
        angle = place * inv_ref[...]
        low = lax.broadcasted_iota(jnp.int32, (count, width), 1) < width // 2
        sin = jnp.sin(angle) * scale
        cosine[pl.ds(at, count), :] = jnp.cos(angle) * scale
        sine[pl.ds(at, count), :] = jnp.where(low, -sin, sin)

    def table(c, _):
        fill(pl.multiple_of(c * half, half), half, base + c * half)
        return 0

    lax.fori_loop(0, 2 * chunks, table, 0)

    def to_end(first, count):
        return ((seq_span * tokens - 1 - first) - lax.broadcasted_iota(
            jnp.int32, (count, width), 0
        )).astype(F32)

    distance = to_end(base + tokens - rows, rows)

    def fading(h, _):
        fade[h] = jnp.exp(decay_ref[h] * distance)
        shrink[h] = jnp.exp(jnp.full((1, vwidth), decay_ref[h] * rows, F32))
        return 0

    lax.fori_loop(0, heads, fading, 0)

    diagonal = lax.broadcasted_iota(jnp.int32, (width, width), 0) == lax.broadcasted_iota(
        jnp.int32, (width, width), 1
    )
    ones = jnp.ones((width, vwidth), BF16)
    queries, next_keys, next_values = (fresh_ref[i].astype(F32) for i in range(3))

    def widen(target, prompt):
        for h in range(heads):
            mine = jnp.zeros((1, width), F32)
            for s in range(SEQS):
                mine = jnp.where(
                    prompt == s, queries[s:s + 1, h * width:(h + 1) * width], mine
                )
            spread = jnp.where(
                diagonal, jnp.broadcast_to(mine, (width, width)), 0.0
            ).astype(BF16)
            target[h] = jnp.dot(spread, ones, preferred_element_type=F32)

    widen(query_wide, sp_place // seq_span)
    for h in range(heads):
        cols = slice(h * width, (h + 1) * width)
        for s in range(SEQS):
            score = jnp.sum(
                queries[s:s + 1, cols] * next_keys[s:s + 1, cols], axis=1, keepdims=True
            )
            own_term[s, h] = score * next_values[s:s + 1, h * vwidth:(h + 1) * vwidth]
        factor[h] = jnp.exp(jnp.full((1, vwidth), decay_ref[h], F32))

    @pl.when(donor)
    def _():
        for part in range(2):
            at = pl.ds(tail_plot[0](part), slip)
            cosine[at, :] = jnp.zeros((slip, width), F32)
            sine[at, :] = jnp.zeros((slip, width), F32)

    @pl.when(host)
    def _():
        settled(1, 2 * slip, guest_sem.at[1])
        for wave in range(2):
            start_all(own_copies(guest_plot, wave))

    send_own(1)

    @pl.when(host)
    def _():
        for part in range(2):
            first = guest_base + tail_plot[0](part)
            fill(guest_plot[0](part), slip, first)
            gap = to_end(first, slip)
            for h in range(heads):
                guest_fade[h, pl.ds(part * slip, slip), :] = jnp.exp(decay_ref[h] * gap)
        widen(guest_wide, guest_place // seq_span)

    def outgoing(g, state, state_to, gist, gist_to, semaphores, at):
        piece = pl.ds(g * pair, pair)
        out = []
        for peer in sp_peers:
            for k, (source, target) in enumerate((
                (gist.at[piece], gist_to.at[sp_place, piece]),
                (state.at[peer, piece], state_to.at[sp_place, piece]),
            )):
                out.append(pltpu.make_async_remote_copy(
                    src_ref=source,
                    dst_ref=target,
                    send_sem=semaphores.at[at + 2 * k],
                    recv_sem=semaphores.at[at + 2 * k + 1],
                    device_id={"sp": peer},
                    device_id_type=MESH,
                ))
        return out

    pltpu.make_async_copy(w_ref, w_ref, local_sem.at[6]).wait()
    wk, wv = w_ref.at[0], w_ref.at[1]

    def partial(at, blocks, w, cols):
        total = None
        for block in blocks:
            depth = pl.ds(pl.multiple_of(block * feats, feats), feats)
            term = jnp.dot(gx[block, at, :], w[depth, cols], preferred_element_type=F32)
            total = term if total is None else total + term
        return total

    def columns(g):
        return (
            pl.ds(pl.multiple_of(g * pair * width, pair * width), pair * width),
            pl.ds(pl.multiple_of(g * pair * vwidth, pair * vwidth), pair * vwidth),
        )

    def chunk_rows(c):
        return pl.ds(pl.multiple_of(c * rows, rows), rows)

    guest_rows = pl.ds(tokens, 2 * slip)

    def begin(at):
        def step(g, _):
            kcols, vcols = columns(g)
            acc_k[at, kcols] = partial(at, early_blocks, wk, kcols)
            acc_v[at, vcols] = partial(at, early_blocks, wv, vcols)
            return 0

        lax.fori_loop(0, groups, step, 0)

    def early(c, _):
        arrived(chunk_plot(c, half), 1)
        begin(chunk_rows(c))
        return 0

    def finish(at, count, weigh, keep, after):
        some = pl.ds(0, count)

        def multiply(g):
            kcols = pl.ds(g * pair * width, pair * width)
            vcols = pl.ds(g * pair * vwidth, pair * vwidth)
            k_tmp[g, some, :] = partial(at, late_blocks, wk, kcols) + acc_k[at, kcols]
            v_tmp[g, some, :] = (
                partial(at, late_blocks, wv, vcols) + acc_v[at, vcols]
            ).astype(BF16)

        def absorb(g):
            for j in range(pair):
                kh = k_tmp[g, some, j * width:(j + 1) * width]
                turned = kh * cosine[at, :] + pltpu.roll(kh, width // 2, 1) * sine[at, :]
                keep(g * pair + j, lax.dot_general(
                    (turned * weigh[g * pair + j]).astype(BF16),
                    v_tmp[g, some, j * vwidth:(j + 1) * vwidth],
                    (((0,), (0,)), ((), ())), preferred_element_type=F32,
                ))
            after(g)

        multiply(0)
        for g in range(1, groups):
            multiply(g)
            absorb(g - 1)
        absorb(groups - 1)

    def keep_on(h, update):
        state_ref[h] = state_ref[h] * shrink[h] + update

    def late(c, _):
        arrived(chunk_plot(c, half), 2)
        finish(chunk_rows(c), rows, fade, keep_on, lambda g: None)
        return 0

    def cut_up(h, held, wide, state, gist):
        for d in range(sp_size):
            state[d, h] = held[d * kept:(d + 1) * kept, :].astype(BF16)
        gist[h] = jnp.sum(wide[h] * held, axis=0, keepdims=True)

    middle = chunks // 2
    lax.fori_loop(LEAD, middle, pass_on_loop, 0)

    @pl.when(host)
    def _():
        arrived(guest_plot, 1)
        pass_on(guest_plot)

    lax.fori_loop(middle, last, pass_on_loop, 0)
    pass_on(last_plot)
    pl.when(full)(functools.partial(pass_on, tail_plot))
    pl.when(host)(functools.partial(begin, guest_rows))
    lax.fori_loop(0, last, early, 0)
    arrived(last_plot, 1)
    pl.when(full)(functools.partial(arrived, tail_plot, 1))
    begin(chunk_rows(last))

    lax.fori_loop(0, middle, late, 0)
    expect(ready_sem, sp_size - above)

    @pl.when(host)
    def _():
        arrived(guest_plot, 2)
        finish(
            guest_rows, 2 * slip, guest_fade,
            lambda h, held: cut_up(h, held, guest_wide, guest_staged, guest_read),
            lambda g: start_all(outgoing(
                g, guest_staged, guest_landed, guest_read, guest_reads, guest_sem, 2
            )),
        )
        guest_landed[sp_place] = guest_staged[sp_place]
        guest_reads[sp_place] = guest_read[...]

    lax.fori_loop(middle, last, late, 0)
    for slot in range(fan):
        settled(1, tokens - 2 * slip, send_sem.at[slot])
    arrived(last_plot, 2)
    pl.when(full)(functools.partial(arrived, tail_plot, 2))
    finish(
        chunk_rows(last), rows, fade,
        lambda h, update: cut_up(
            h, state_ref[h] * shrink[h] + update, query_wide, staged, read
        ),
        lambda g: start_all(outgoing(g, staged, landed, read, reads, out_sem, 0)),
    )

    landed[sp_place] = staged[sp_place]
    reads[sp_place] = read[...]
    for slot in range(fan):
        settled(side - 1, tokens // 2 - slip, send_sem.at[fan + slot])
    moved = (4 * (side - 1) + 2 * (side - 1) ** 2) * slip
    pl.when(full)(functools.partial(settled, 1, moved, slip_send.at[0]))
    pl.when(donor)(functools.partial(settled, 1, 2 * slip, guest_sem.at[0]))
    pl.when(host)(functools.partial(settled, 1, moved, slip_send.at[1]))

    def exchanged(gist, state, count, semaphores, at):
        some = pl.ds(0, count)
        for k, target in enumerate((gist, state)):
            pltpu.make_async_copy(
                target.at[some], target.at[some], semaphores.at[at + 2 * k]
            ).wait()

    pl.when(host)(functools.partial(exchanged, guest_reads, guest_landed, 1, guest_sem, 3))
    pl.when(jnp.logical_not(host))(
        functools.partial(exchanged, guest_reads, guest_landed, 2, guest_sem, 3)
    )
    exchanged(reads, landed, sp_size - 1, out_sem, 1)
    row = lax.broadcasted_iota(jnp.int32, (SEQS, heads * vwidth), 0)
    out = jnp.zeros((SEQS, heads * vwidth), F32)
    for s in range(SEQS):
        members = range(s * seq_span, (s + 1) * seq_span)
        guests = range(2) if s == SEQS - 1 else ()
        carried = functools.reduce(
            jnp.add, [reads[m] for m in members] + [guest_reads[m] for m in guests]
        )
        mixed = factor[...] * carried + own_term[s]
        normed = mixed * lax.rsqrt(jnp.mean(mixed * mixed, axis=2, keepdims=True) + 1e-06)
        line = jnp.concatenate([normed[h] for h in range(heads)], axis=1) * gain_ref[...]
        out = jnp.where(row == s, jnp.broadcast_to(line, out.shape), out)
        for h in range(heads):
            cache_ref[s, h] = functools.reduce(
                jnp.add,
                [landed[m, h].astype(F32) for m in members]
                + [guest_landed[m, h].astype(F32) for m in guests],
            ).astype(BF16)
    first_ref[...] = out.astype(BF16)
    exchanged(reads, landed, sp_size - 1, out_sem, 0)

    @pl.when(host)
    def _():
        exchanged(reads, guest_staged, sp_size - 1, guest_sem, 2)


def settle(cache_ref, first_ref, cache_out, first_out):
    cache_out[...] = cache_ref[...]
    first_out[...] = first_ref[...]


def on_device(
    layer_input, key_weight, value_weight, decay_exponent, query_new, key_new, value_new, norm_gain
):
    tokens, feats = layer_input.shape
    parts = lax.axis_size("tp")
    sp_size = lax.axis_size("sp")
    seq_span = sp_size // SEQS
    side = math.isqrt(parts)
    heads = decay_exponent.shape[0]
    width = key_weight.shape[1] // heads
    vwidth = value_weight.shape[1] // heads
    kept = width // sp_size
    room = tokens + 2 * SLIP
    groups = heads // next(p for p in (4, 2, 1) if heads % p == 0)
    steps = np.linspace(0.0, 1.0, width // 2, dtype=np.float32)
    inverse = (np.float32(1.0) / np.power(np.float32(10000.0), steps)).astype(np.float32)
    inverse = jnp.asarray(np.concatenate([inverse, inverse])[None, :])
    anywhere = pl.BlockSpec(memory_space=pltpu.HBM)
    vmem = pl.BlockSpec(memory_space=pltpu.VMEM)
    held = [
        pltpu.with_memory_space_constraint(part, pltpu.HBM)
        for part in (
            decay_exponent, inverse, query_new, key_new, value_new, norm_gain.reshape(1, -1),
            layer_input, key_weight, value_weight,
        )
    ]
    state_cache, first_read = pl.pallas_call(
        functools.partial(gather_kernel, side, seq_span, CHUNKS),
        out_shape=(
            jax.ShapeDtypeStruct((SEQS, heads, kept, vwidth), BF16),
            jax.ShapeDtypeStruct((SEQS, heads * vwidth), BF16),
        ),
        in_specs=[anywhere] * 9,
        out_specs=(vmem, vmem),
        scratch_shapes=[
            pltpu.SMEM((heads,), F32),
            pltpu.VMEM(inverse.shape, F32),
            pltpu.VMEM((3,) + query_new.shape, BF16),
            pltpu.VMEM((1, heads * vwidth), F32),
            pltpu.VMEM((parts, room, feats), BF16),
            pltpu.VMEM((2,) + key_weight.shape, BF16),
            pltpu.VMEM((room, width), F32),
            pltpu.VMEM((room, width), F32),
            pltpu.VMEM((room, heads * width), F32),
            pltpu.VMEM((room, heads * vwidth), F32),
            pltpu.VMEM((heads, width, vwidth), F32),
            pltpu.VMEM((heads, tokens // CHUNKS, width), F32),
            pltpu.VMEM((heads, 1, vwidth), F32),
            pltpu.VMEM((heads, width, vwidth), F32),
            pltpu.VMEM((SEQS, heads, 1, vwidth), F32),
            pltpu.VMEM((heads, 1, vwidth), F32),
            pltpu.VMEM((sp_size, heads, kept, vwidth), BF16),
            pltpu.VMEM((sp_size, heads, kept, vwidth), BF16),
            pltpu.VMEM((heads, 1, vwidth), F32),
            pltpu.VMEM((sp_size, heads, 1, vwidth), F32),
            pltpu.VMEM((groups, tokens // CHUNKS, heads // groups * width), F32),
            pltpu.VMEM((groups, tokens // CHUNKS, heads // groups * vwidth), BF16),
            pltpu.VMEM((heads, 2 * SLIP, width), F32),
            pltpu.VMEM((heads, width, vwidth), F32),
            pltpu.VMEM((sp_size, heads, kept, vwidth), BF16),
            pltpu.VMEM((2, heads, kept, vwidth), BF16),
            pltpu.VMEM((heads, 1, vwidth), F32),
            pltpu.VMEM((2, heads, 1, vwidth), F32),
            pltpu.SemaphoreType.DMA((4 * (side - 1),)),
            pltpu.SemaphoreType.DMA((3, CHUNKS)),
            pltpu.SemaphoreType.DMA((2,)),
            pltpu.SemaphoreType.DMA((2, 3)),
            pltpu.SemaphoreType.DMA((7,)),
            pltpu.SemaphoreType.DMA((4,)),
            pltpu.SemaphoreType.DMA((6,)),
            pltpu.SemaphoreType.REGULAR,
            pltpu.SemaphoreType.REGULAR,
            pltpu.SemaphoreType.REGULAR,
            pltpu.SemaphoreType.REGULAR,
            pltpu.SemaphoreType.REGULAR,
        ],
        compiler_params=pltpu.CompilerParams(
            collective_id=0, has_side_effects=True, vmem_limit_bytes=VMEM_KIB * 1024
        ),
    )(*held)
    return pl.pallas_call(
        settle,
        out_shape=(
            jax.ShapeDtypeStruct(state_cache.shape, BF16),
            jax.ShapeDtypeStruct(first_read.shape, BF16),
        ),
        in_specs=[vmem, vmem],
        out_specs=(vmem, vmem),
        compiler_params=pltpu.CompilerParams(vmem_limit_bytes=4 * 1024 * 1024),
    )(state_cache, first_read)


def solution(mesh):
    in_specs = (
        P("sp", "tp"),
        P(None, "tp"),
        P(None, "tp"),
        P("tp"),
        P(None, "tp"),
        P(None, "tp"),
        P(None, "tp"),
        P("tp"),
    )
    out_specs = (P(None, "tp", "sp", None), P(None, "tp"))
    return jax.shard_map(
        on_device, mesh=mesh, in_specs=in_specs, out_specs=out_specs, check_vma=False
    )
```

time: 81.7 us -> 81 us (level)
  no operation moved by 1% of the time
where the time goes in v4:
time: 81 us; the launch traced here: 80.9 us
  Pallas kernels  80.2 us (99%)
    pallas_call x1, Pallas kernels, on_device(): pl.pallas_call(functools.partial(gather_kernel, side, seq_span, CHUNKS),...  79.6 us

profile of v4, /device:TPU:0, one launch (start us, length us, event | category | flops | bytes accessed | tf_op | source)
XLA Modules:
  0.0 80.9 jit_solution(9849353445370288739)
XLA Ops:
  0.6 79.6 %shard_map.104 = (bf16[2,8,16,128]{3,2,1,0:T(8,128)(2,1)S(1)}, bf16[2,1024]{1,0:T(2,128)(2,1)S(1)}) custom-call(f32[8]{0:T(128)} %decay_hbm.1, f32[1,128]{1,0:T(1,128)} %constant.2.clone.inv_hbm, bf16[2,1024]{1,0:T(2,128)(2,1)} %query_hbm.1, bf16[2,1024]{1,0:T(2,128)(2,1)} %key_hbm.1, bf16[2,1024]{1,0:T(2,128)(2,1)} %value_hbm.1, f32[1,1024]{1,0:T(1,128)} %bitcast.1, ...), custom_call_target="tpu_custom_call" | custom-call | tf_op jit(solution)/shard_map/pallas_call | solution.py:575
  80.2 0.6 shard_map.105

commit v5 on v4

--- a/solution.py
+++ b/solution.py
@@ -10,7 +10,7 @@
 from jax.sharding import PartitionSpec as P
 
 SEQS = 2
-CHUNKS = 8
+CHUNKS = (1, 1, 2, 2, 1, 1)
 LEAD = 1
 SLIP = 16
 VMEM_KIB = 48 * 1024
@@ -20,7 +20,7 @@
 
 
 def gather_kernel(
-    side, seq_span, chunks,
+    side, seq_span,
     decay_hbm, inv_hbm, query_hbm, key_hbm, value_hbm, gain_hbm, x_ref, wk_ref, wv_ref,
     cache_ref, first_ref,
     decay_ref, inv_ref, fresh_ref, gain_ref,
@@ -31,10 +31,13 @@
     go_sem, ready_sem, x_sem, y_sem, mate_sem,
 ):
     tokens, feats = x_ref.shape
-    rows = tokens // chunks
-    half = rows // 2
+    unit = tokens // sum(CHUNKS)
+    sizes = [unit * n for n in CHUNKS]
     slip = SLIP
-    last = chunks - 1
+    ahead = 2 * slip
+    starts = [ahead + unit * sum(CHUNKS[:c]) for c in range(len(CHUNKS))]
+    longest = max(sizes)
+    last = len(CHUNKS) - 1
     heads, width, vwidth = state_ref.shape
     pair = next(p for p in (4, 2, 1) if heads % p == 0)
     me = lax.axis_index("tp")
@@ -66,8 +69,11 @@
     early_blocks = [me] + x_peers + y_peers
 
     def fetch(first):
-        at = pl.ds(0, rows) if first else pl.ds(rows, tokens - rows)
-        return pltpu.make_async_copy(x_ref.at[at], gx.at[me, at], local_sem.at[0 if first else 1])
+        start, count = (0, sizes[0]) if first else (sizes[0], tokens - sizes[0])
+        return pltpu.make_async_copy(
+            x_ref.at[pl.ds(start, count)], gx.at[me, pl.ds(ahead + start, count)],
+            local_sem.at[0 if first else 1],
+        )
 
     fetch(True).start()
     barrier = pltpu.get_barrier_semaphore()
@@ -111,19 +117,22 @@
         tell(ready_sem, "sp", peer)
         return 0
 
-    def chunk_plot(c, count):
+    def chunk_plot(c):
+        half = sizes[c] // 2
         return (
-            lambda part: pl.multiple_of(c * rows + part * half, half),
-            count, lambda slot: send_sem.at[slot], lambda kind: recv_sem.at[kind, c],
+            lambda part: starts[c] + part * half,
+            half - slip if c == last else half,
+            lambda slot: send_sem.at[slot], lambda kind: recv_sem.at[kind, c],
         )
 
     def slip_plot(which):
         return (
-            lambda part: tokens + part * slip if which else last * rows + (part + 1) * half - slip,
+            lambda part: part * slip if which else starts[last] + (part + 1) * (sizes[last] // 2) - slip,
             slip, lambda slot: slip_send.at[which], lambda kind: slip_recv.at[which, kind],
         )
 
-    last_plot, tail_plot, guest_plot = chunk_plot(last, half - slip), slip_plot(0), slip_plot(1)
+    plots = [chunk_plot(c) for c in range(last + 1)]
+    tail_plot, guest_plot = slip_plot(0), slip_plot(1)
 
     def remote(plot, slot, block, part, target, kind):
         start, count, send, recv = plot
@@ -190,7 +199,7 @@
         pl.semaphore_wait(go_sem, 1)
 
     def send_first(on_x):
-        start_all(along(chunk_plot(0, half), 0, on_x))
+        start_all(along(plots[0], 0, on_x))
 
     x_last, y_last = my_x == side - 1, my_y == side - 1
     pl.when(x_last)(functools.partial(send_first, True))
@@ -216,12 +225,8 @@
                 gx[block, pl.ds(tail_plot[0](part), slip), :] = jnp.zeros((slip, feats), BF16)
 
     def send_own(wave):
-        def body(c, _):
-            start_all(own_copies(chunk_plot(c, half), wave))
-            return 0
-
-        lax.fori_loop(1 - wave, last, body, 0)
-        start_all(own_copies(last_plot, wave))
+        for plot in plots[1 - wave:]:
+            start_all(own_copies(plot, wave))
 
         @pl.when(full)
         def _():
@@ -253,11 +258,8 @@
         arrived(plot, 0)
         start_all(relay_copies(plot))
 
-    def pass_on_loop(c, _):
-        pass_on(chunk_plot(c, half))
-        return 0
-
-    lax.fori_loop(0, LEAD, pass_on_loop, 0)
+    for plot in plots[:LEAD]:
+        pass_on(plot)
 
     @pl.when(core == 0)
     def _():
@@ -281,21 +283,24 @@
         sine[pl.ds(at, count), :] = jnp.where(low, -sin, sin)
 
     def table(c, _):
-        fill(pl.multiple_of(c * half, half), half, base + c * half)
+        at = pl.multiple_of(ahead + c * (unit // 2), math.gcd(ahead, unit // 2))
+        fill(at, unit // 2, base + c * (unit // 2))
         return 0
 
-    lax.fori_loop(0, 2 * chunks, table, 0)
+    lax.fori_loop(0, 2 * sum(CHUNKS), table, 0)
 
     def to_end(first, count):
         return ((seq_span * tokens - 1 - first) - lax.broadcasted_iota(
             jnp.int32, (count, width), 0
         )).astype(F32)
 
-    distance = to_end(base + tokens - rows, rows)
+    distance = to_end(base + tokens - longest, longest)
+    spans = sorted(set(CHUNKS))
 
     def fading(h, _):
         fade[h] = jnp.exp(decay_ref[h] * distance)
-        shrink[h] = jnp.exp(jnp.full((1, vwidth), decay_ref[h] * rows, F32))
+        for k, n in enumerate(spans):
+            shrink[k, h] = jnp.exp(jnp.full((1, vwidth), decay_ref[h] * (unit * n), F32))
         return 0
 
     lax.fori_loop(0, heads, fading, 0)
@@ -346,17 +351,17 @@
     @pl.when(host)
     def _():
         for part in range(2):
-            first = guest_base + tail_plot[0](part)
+            first = guest_base + tail_plot[0](part) - ahead
             fill(guest_plot[0](part), slip, first)
             gap = to_end(first, slip)
             for h in range(heads):
                 guest_fade[h, pl.ds(part * slip, slip), :] = jnp.exp(decay_ref[h] * gap)
         widen(guest_wide, guest_place // seq_span)
 
-    def outgoing(g, state, state_to, gist, gist_to, semaphores, at):
+    def outgoing(g, state, state_to, gist, gist_to, semaphores, at, peers=None):
         piece = pl.ds(g * pair, pair)
         out = []
-        for peer in sp_peers:
+        for peer in peers or sp_peers:
             for k, (source, target) in enumerate((
                 (gist.at[piece], gist_to.at[sp_place, piece]),
                 (state.at[peer, piece], state_to.at[sp_place, piece]),
@@ -389,9 +394,9 @@
         )
 
     def chunk_rows(c):
-        return pl.ds(pl.multiple_of(c * rows, rows), rows)
-
-    guest_rows = pl.ds(tokens, 2 * slip)
+        return pl.ds(starts[c], sizes[c])
+
+    first_rows = pl.ds(0, starts[0] + sizes[0])
 
     def begin(at):
         def step(g, _):
@@ -402,96 +407,102 @@
 
         lax.fori_loop(0, groups, step, 0)
 
-    def early(c, _):
-        arrived(chunk_plot(c, half), 1)
-        begin(chunk_rows(c))
-        return 0
-
-    def finish(at, count, weigh, keep, after):
-        some = pl.ds(0, count)
-
-        def multiply(g):
-            kcols = pl.ds(g * pair * width, pair * width)
-            vcols = pl.ds(g * pair * vwidth, pair * vwidth)
-            k_tmp[g, some, :] = partial(at, late_blocks, wk, kcols) + acc_k[at, kcols]
-            v_tmp[g, some, :] = (
-                partial(at, late_blocks, wv, vcols) + acc_v[at, vcols]
-            ).astype(BF16)
-
-        def absorb(g):
-            for j in range(pair):
-                kh = k_tmp[g, some, j * width:(j + 1) * width]
-                turned = kh * cosine[at, :] + pltpu.roll(kh, width // 2, 1) * sine[at, :]
-                keep(g * pair + j, lax.dot_general(
-                    (turned * weigh[g * pair + j]).astype(BF16),
-                    v_tmp[g, some, j * vwidth:(j + 1) * vwidth],
-                    (((0,), (0,)), ((), ())), preferred_element_type=F32,
-                ))
-            after(g)
-
-        multiply(0)
-        for g in range(1, groups):
-            multiply(g)
-            absorb(g - 1)
-        absorb(groups - 1)
-
-    def keep_on(h, update):
-        state_ref[h] = state_ref[h] * shrink[h] + update
-
-    def late(c, _):
-        arrived(chunk_plot(c, half), 2)
-        finish(chunk_rows(c), rows, fade, keep_on, lambda g: None)
-        return 0
+    def multiply(g, at):
+        some = pl.ds(0, at.size)
+        kcols = pl.ds(g * pair * width, pair * width)
+        vcols = pl.ds(g * pair * vwidth, pair * vwidth)
+        k_tmp[g, some, :] = partial(at, late_blocks, wk, kcols) + acc_k[at, kcols]
+        v_tmp[g, some, :] = (
+            partial(at, late_blocks, wv, vcols) + acc_v[at, vcols]
+        ).astype(BF16)
+
+    def absorb(g, at, some, weigh, keep):
+        past = weigh.shape[1] - at.size
+        for j in range(pair):
+            kh = k_tmp[g, some, j * width:(j + 1) * width]
+            turned = kh * cosine[at, :] + pltpu.roll(kh, width // 2, 1) * sine[at, :]
+            keep(g * pair + j, lax.dot_general(
+                (turned * weigh[g * pair + j, past:, :]).astype(BF16),
+                v_tmp[g, some, j * vwidth:(j + 1) * vwidth],
+                (((0,), (0,)), ((), ())), preferred_element_type=F32,
+            ))
+
+    def finish(c, keep, after):
+        at = chunk_rows(c)
+        every, some = (at, pl.ds(0, sizes[c])) if c else (first_rows, at)
+        multiply(0, every)
+        for g in range(1, groups + 1):
+            if g < groups:
+                multiply(g, every)
+            absorb(g - 1, at, some, fade, keep)
+            after(g - 1)
+
+    def carry_on(c, h, update):
+        return state_ref[h] * shrink[spans.index(CHUNKS[c]), h] + update
+
+    def late(c):
+        def keep(h, update):
+            state_ref[h] = carry_on(c, h, update)
+
+        arrived(plots[c], 2)
+        finish(c, keep, lambda g: None)
 
     def cut_up(h, held, wide, state, gist):
         for d in range(sp_size):
             state[d, h] = held[d * kept:(d + 1) * kept, :].astype(BF16)
         gist[h] = jnp.sum(wide[h] * held, axis=0, keepdims=True)
 
-    middle = chunks // 2
-    lax.fori_loop(LEAD, middle, pass_on_loop, 0)
+    middle = LEAD
+    for plot in plots[LEAD:middle]:
+        pass_on(plot)
+
+    pl.when(host)(functools.partial(pass_on, guest_plot))
+    for plot in plots[middle:]:
+        pass_on(plot)
+    pl.when(full)(functools.partial(pass_on, tail_plot))
+    pl.when(host)(functools.partial(arrived, guest_plot, 1))
+    for c, plot in enumerate(plots):
+        arrived(plot, 1)
+        if c == last:
+            pl.when(full)(functools.partial(arrived, tail_plot, 1))
+        begin(chunk_rows(c) if c else first_rows)
+    expect(ready_sem, sp_size - above)
+
+    pl.when(host)(functools.partial(arrived, guest_plot, 2))
+    late(0)
 
     @pl.when(host)
     def _():
-        arrived(guest_plot, 1)
-        pass_on(guest_plot)
-
-    lax.fori_loop(middle, last, pass_on_loop, 0)
-    pass_on(last_plot)
-    pl.when(full)(functools.partial(pass_on, tail_plot))
-    pl.when(host)(functools.partial(begin, guest_rows))
-    lax.fori_loop(0, last, early, 0)
-    arrived(last_plot, 1)
-    pl.when(full)(functools.partial(arrived, tail_plot, 1))
-    begin(chunk_rows(last))
-
-    lax.fori_loop(0, middle, late, 0)
-    expect(ready_sem, sp_size - above)
-
-    @pl.when(host)
-    def _():
-        arrived(guest_plot, 2)
-        finish(
-            guest_rows, 2 * slip, guest_fade,
-            lambda h, held: cut_up(h, held, guest_wide, guest_staged, guest_read),
-            lambda g: start_all(outgoing(
+        guest_rows = pl.ds(0, ahead)
+        for g in range(groups):
+            absorb(
+                g, guest_rows, guest_rows, guest_fade,
+                lambda h, held: cut_up(h, held, guest_wide, guest_staged, guest_read),
+            )
+            start_all(outgoing(
                 g, guest_staged, guest_landed, guest_read, guest_reads, guest_sem, 2
-            )),
-        )
+            ))
         guest_landed[sp_place] = guest_staged[sp_place]
         guest_reads[sp_place] = guest_read[...]
 
-    lax.fori_loop(middle, last, late, 0)
+    for c in range(1, last):
+        late(c)
+
+    def deal(g):
+        to = (staged, landed, read, reads, out_sem, 0)
+        start_all(outgoing(g, *to, sp_peers[:2]))
+        if g == groups - 1:
+            for k in range(groups):
+                start_all(outgoing(k, *to, sp_peers[2:]))
+
     for slot in range(fan):
         settled(1, tokens - 2 * slip, send_sem.at[slot])
-    arrived(last_plot, 2)
+    arrived(plots[last], 2)
     pl.when(full)(functools.partial(arrived, tail_plot, 2))
     finish(
-        chunk_rows(last), rows, fade,
-        lambda h, update: cut_up(
-            h, state_ref[h] * shrink[h] + update, query_wide, staged, read
-        ),
-        lambda g: start_all(outgoing(g, staged, landed, read, reads, out_sem, 0)),
+        last,
+        lambda h, update: cut_up(h, carry_on(last, h, update), query_wide, staged, read),
+        deal,
     )
 
     landed[sp_place] = staged[sp_place]
@@ -559,6 +570,7 @@
     vwidth = value_weight.shape[1] // heads
     kept = width // sp_size
     room = tokens + 2 * SLIP
+    longest = tokens // sum(CHUNKS) * max(CHUNKS)
     groups = heads // next(p for p in (4, 2, 1) if heads % p == 0)
     steps = np.linspace(0.0, 1.0, width // 2, dtype=np.float32)
     inverse = (np.float32(1.0) / np.power(np.float32(10000.0), steps)).astype(np.float32)
@@ -573,7 +585,7 @@
         )
     ]
     state_cache, first_read = pl.pallas_call(
-        functools.partial(gather_kernel, side, seq_span, CHUNKS),
+        functools.partial(gather_kernel, side, seq_span),
         out_shape=(
             jax.ShapeDtypeStruct((SEQS, heads, kept, vwidth), BF16),
             jax.ShapeDtypeStruct((SEQS, heads * vwidth), BF16),
@@ -592,8 +604,8 @@
             pltpu.VMEM((room, heads * width), F32),
             pltpu.VMEM((room, heads * vwidth), F32),
             pltpu.VMEM((heads, width, vwidth), F32),
-            pltpu.VMEM((heads, tokens // CHUNKS, width), F32),
-            pltpu.VMEM((heads, 1, vwidth), F32),
+            pltpu.VMEM((heads, longest, width), F32),
+            pltpu.VMEM((len(set(CHUNKS)), heads, 1, vwidth), F32),
             pltpu.VMEM((heads, width, vwidth), F32),
             pltpu.VMEM((SEQS, heads, 1, vwidth), F32),
             pltpu.VMEM((heads, 1, vwidth), F32),
@@ -601,8 +613,8 @@
             pltpu.VMEM((sp_size, heads, kept, vwidth), BF16),
             pltpu.VMEM((heads, 1, vwidth), F32),
             pltpu.VMEM((sp_size, heads, 1, vwidth), F32),
-            pltpu.VMEM((groups, tokens // CHUNKS, heads // groups * width), F32),
-            pltpu.VMEM((groups, tokens // CHUNKS, heads // groups * vwidth), BF16),
+            pltpu.VMEM((groups, longest, heads // groups * width), F32),
+            pltpu.VMEM((groups, longest, heads // groups * vwidth), BF16),
             pltpu.VMEM((heads, 2 * SLIP, width), F32),
             pltpu.VMEM((heads, width, vwidth), F32),
             pltpu.VMEM((sp_size, heads, kept, vwidth), BF16),
@@ -610,7 +622,7 @@
             pltpu.VMEM((heads, 1, vwidth), F32),
             pltpu.VMEM((2, heads, 1, vwidth), F32),
             pltpu.SemaphoreType.DMA((4 * (side - 1),)),
-            pltpu.SemaphoreType.DMA((3, CHUNKS)),
+            pltpu.SemaphoreType.DMA((3, len(CHUNKS))),
             pltpu.SemaphoreType.DMA((2,)),
             pltpu.SemaphoreType.DMA((2, 3)),
             pltpu.SemaphoreType.DMA((7,)),

time: 81 us -> 80.7 us (level)
  no operation moved by 1% of the time
where the time goes in v5:
time: 80.7 us; the launch traced here: 80.1 us
  Pallas kernels  79.5 us (99%)
    pallas_call x1, Pallas kernels, on_device(): pl.pallas_call(functools.partial(gather_kernel, side, seq_span), out_shap...  78.9 us

profile of v5, /device:TPU:0, one launch (start us, length us, event | category | flops | bytes accessed | tf_op | source)
XLA Modules:
  0.0 80.1 jit_solution(4171008250576980811)
XLA Ops:
  0.6 78.9 %shard_map.104 = (bf16[2,8,16,128]{3,2,1,0:T(8,128)(2,1)S(1)}, bf16[2,1024]{1,0:T(2,128)(2,1)S(1)}) custom-call(f32[8]{0:T(128)} %decay_hbm.1, f32[1,128]{1,0:T(1,128)} %constant.2.clone.inv_hbm, bf16[2,1024]{1,0:T(2,128)(2,1)} %query_hbm.1, bf16[2,1024]{1,0:T(2,128)(2,1)} %key_hbm.1, bf16[2,1024]{1,0:T(2,128)(2,1)} %value_hbm.1, f32[1,1024]{1,0:T(1,128)} %bitcast.1, ...), custom_call_target="tpu_custom_call" | custom-call | tf_op jit(solution)/shard_map/pallas_call | solution.py:587
  79.5 0.6 shard_map.105

commit v6 on v5

--- a/solution.py
+++ b/solution.py
@@ -363,9 +363,11 @@
         out = []
         for peer in peers or sp_peers:
             for k, (source, target) in enumerate((
-                (gist.at[piece], gist_to.at[sp_place, piece]),
+                (gist, gist_to.at[sp_place]),
                 (state.at[peer, piece], state_to.at[sp_place, piece]),
             )):
+                if k == 0 and g < groups - 1:
+                    continue
                 out.append(pltpu.make_async_remote_copy(
                     src_ref=source,
                     dst_ref=target,
@@ -432,10 +434,12 @@
         every, some = (at, pl.ds(0, sizes[c])) if c else (first_rows, at)
         multiply(0, every)
         for g in range(1, groups + 1):
-            if g < groups:
+            if g < groups and c < last:
                 multiply(g, every)
             absorb(g - 1, at, some, fade, keep)
             after(g - 1)
+            if g < groups and c == last:
+                multiply(g, every)
 
     def carry_on(c, h, update):
         return state_ref[h] * shrink[spans.index(CHUNKS[c]), h] + update
@@ -490,10 +494,10 @@
 
     def deal(g):
         to = (staged, landed, read, reads, out_sem, 0)
-        start_all(outgoing(g, *to, sp_peers[:2]))
+        start_all(outgoing(g, *to, sp_peers[:4]))
         if g == groups - 1:
             for k in range(groups):
-                start_all(outgoing(k, *to, sp_peers[2:]))
+                start_all(outgoing(k, *to, sp_peers[4:]))
 
     for slot in range(fan):
         settled(1, tokens - 2 * slip, send_sem.at[slot])

time: 80.7 us -> 80.5 us (level)
  no operation moved by 1% of the time
where the time goes in v6:
time: 80.5 us; the launch traced here: 80.3 us
  Pallas kernels  79.6 us (99%)
    pallas_call x1, Pallas kernels, on_device(): pl.pallas_call(functools.partial(gather_kernel, side, seq_span), out_shap...  79 us

profile of v6, /device:TPU:0, one launch (start us, length us, event | category | flops | bytes accessed | tf_op | source)
XLA Modules:
  0.0 80.3 jit_solution(12360076627645809914)
XLA Ops:
  0.6 79.0 %shard_map.104 = (bf16[2,8,16,128]{3,2,1,0:T(8,128)(2,1)S(1)}, bf16[2,1024]{1,0:T(2,128)(2,1)S(1)}) custom-call(f32[8]{0:T(128)} %decay_hbm.1, f32[1,128]{1,0:T(1,128)} %constant.2.clone.inv_hbm, bf16[2,1024]{1,0:T(2,128)(2,1)} %query_hbm.1, bf16[2,1024]{1,0:T(2,128)(2,1)} %key_hbm.1, bf16[2,1024]{1,0:T(2,128)(2,1)} %value_hbm.1, f32[1,1024]{1,0:T(1,128)} %bitcast.1, ...), custom_call_target="tpu_custom_call" | custom-call | tf_op jit(solution)/shard_map/pallas_call | solution.py:591
  79.6 0.6 shard_map.105
